TPU v7x, 256 devices: a whole 4x4x8 slice. The times are simulated.
256 devices in a mesh: ep: 64 (over z, x, core), tp: 4 (over y).
Axes of the slice: x: 4, y: 4, z: 8, core: 2. Of those that a mesh axis runs over, the one named last changes fastest.
Arguments:
- x_attend: bfloat16 [32768, 2048], P('ep'), may hold values from -6 to 6
- attend_gain: float32 [2048], replicated, may hold values from 0.1 to 1.9
- w_query: bfloat16 [2048, 1024], P(None, 'tp'), may hold values from -0.125 to 0.125
- w_key: bfloat16 [2048, 512], P(None, 'tp'), may hold values from -0.125 to 0.125
- w_value: bfloat16 [2048, 512], P(None, 'tp'), may hold values from -0.125 to 0.125
- query_gain: float32 [64], replicated, may hold values from 0.1 to 1.9
- key_gain: float32 [64], replicated, may hold values from 0.1 to 1.9
- sink_logit: float32 [16], P('tp'), may hold values from 4 to 8
- w_output: bfloat16 [1024, 2048], P('tp'), may hold values from -1.5 to 1.5
- x_experts: bfloat16 [24576, 2048], P('ep'), may hold values from -6 to 6
- expert_gain: float32 [2048], replicated, may hold values from 0.1 to 1.9
- routes: int32 [24576, 2], P('ep'), may hold values from 0 to 63, all different within a row; in each aligned block of 384 rows (0 to 383, 384 to 767, ...) at most 18 rows name the same one
- group_prob: float32 [24576], P('ep'), may hold values from 0.3 to 1
- expert_prob: float32 [24576, 2], P('ep'), may hold values from 0.05 to 1
- w_gate: bfloat16 [64, 2048, 1024], P('ep', None, 'tp'), may hold values from -0.125 to 0.125
- w_up: bfloat16 [64, 2048, 1024], P('ep', None, 'tp'), may hold values from -0.125 to 0.125
- w_down: bfloat16 [64, 1024, 2048], P('ep', 'tp'), may hold values from -0.1875 to 0.1875
Outputs:
- attend_out: bfloat16 [32768, 2048], P(('ep', 'tp'))
- expert_out: bfloat16 [24576, 2048], P('ep', 'tp')
Inputs may be any that keep to these rules, and one draw needn't show every extreme that they name: `routes`: each row names 2 different experts. Among the rows of one device no expert is named more than 18 times, and in every draw some expert is named exactly 18 times by one device's rows.
All inputs are finite; a program needn't handle non-finite values.
Results may differ from a plain program's by a relative error of at most 0.012.
Values may be sent and summed in bfloat16 or wider, within the bound.
A program may use at most 64 MiB of HBM per device.

v0:
```python
import jax
import jax.numpy as jnp
from jax import lax
from jax.sharding import PartitionSpec as P

HEAD_DIM = 64
WINDOW = 128
GRID_W = 64


epsilon = 1e-06
rope_base = 10000.0


def extended(x, sides, width):
    for axis, dim in sides:
        peers, length = (lax.axis_size(axis), x.shape[dim])
        up = [(i, (i + 1) % peers) for i in range(peers - 1)]
        down = [(j, i) for i, j in up]
        last = lax.slice_in_dim(x, length - width, length, axis=dim)
        initial = lax.slice_in_dim(x, 0, width, axis=dim)
        before = lax.ppermute(last, axis, up)
        after = lax.ppermute(initial, axis, down)
        x = jnp.concatenate([before, x, after], axis=dim)
    return x


def joined_along(parts, dim):
    shape = list(parts.shape[1:])
    shape[dim] *= parts.shape[0]
    return jnp.moveaxis(parts, 0, dim).reshape(shape)


def sent_to_all(x, axis):
    copies = jnp.broadcast_to(x, (lax.axis_size(axis), *x.shape))
    return lax.all_to_all(copies, axis, split_axis=0, concat_axis=0, tiled=True)


def collect(x, axis, dim):
    return joined_along(sent_to_all(x, axis), dim)


def rms_scale(inputs, gain):
    values_f = inputs.astype(jnp.float32)
    scaled = values_f * lax.rsqrt(jnp.mean(values_f * values_f, axis=-1, keepdims=True) + epsilon)
    return (scaled * gain).astype(jnp.bfloat16)


def rope_tables(positions):
    grid_rows = (positions // GRID_W).astype(jnp.float32)
    grid_cols = (positions % GRID_W).astype(jnp.float32)
    half_dim = HEAD_DIM // 2
    inverse = rope_base ** (-jnp.arange(0, half_dim, 2, dtype=jnp.float32) / half_dim)
    angles = jnp.concatenate([grid_rows[:, None] * inverse, grid_cols[:, None] * inverse], axis=-1)
    return (jnp.cos(angles), jnp.sin(angles))


def head_norm_rope(projected, gain, cosine, sine_tab):
    scaled = (
        projected
        * lax.rsqrt(jnp.mean(projected * projected, axis=-1, keepdims=True) + epsilon)
        * gain
    )
    first_half, second_half = jnp.split(scaled, 2, axis=-1)
    cos_b = cosine[:, None, :]
    sin_b = sine_tab[:, None, :]
    turned = jnp.concatenate(
        [first_half * cos_b - second_half * sin_b, second_half * cos_b + first_half * sin_b],
        axis=-1,
    )
    return turned.astype(jnp.bfloat16)


def per_device(
    x_attend,
    attend_gain,
    w_query,
    w_key,
    w_value,
    query_gain,
    key_gain,
    sink_logit,
    w_output,
    x_experts,
    expert_gain,
    routes,
    group_prob,
    expert_prob,
    w_gate,
    w_up,
    w_down,
):
    tok_rows = x_attend.shape[0]
    model_width = x_attend.shape[1]
    heads_local = sink_logit.shape[0]
    kv_local = w_key.shape[1] // HEAD_DIM
    group = heads_local // kv_local
    offset = lax.axis_index("ep") * tok_rows
    positions = offset + jnp.arange(tok_rows, dtype=jnp.int32)
    cosine, sine_tab = rope_tables(positions)
    normed = rms_scale(x_attend, attend_gain)
    queries = head_norm_rope(
        jnp.dot(normed, w_query, preferred_element_type=jnp.float32).reshape(
            tok_rows, heads_local, HEAD_DIM
        ),
        query_gain,
        cosine,
        sine_tab,
    )
    key_rows = head_norm_rope(
        jnp.dot(normed, w_key, preferred_element_type=jnp.float32).reshape(
            tok_rows, kv_local, HEAD_DIM
        ),
        key_gain,
        cosine,
        sine_tab,
    )
    values = jnp.dot(normed, w_value, preferred_element_type=jnp.float32).astype(jnp.bfloat16)
    stacked = jnp.stack([key_rows.reshape(tok_rows, kv_local * HEAD_DIM), values], axis=0)
    padded = extended(stacked, (("ep", 1),), WINDOW)
    span_keys = padded[0].reshape(tok_rows + 2 * WINDOW, kv_local, HEAD_DIM)
    span_values = padded[1].reshape(tok_rows + 2 * WINDOW, kv_local, HEAD_DIM)
    scores = jnp.einsum(
        "qhgd,khd->hgqk",
        queries.reshape(tok_rows, kv_local, group, HEAD_DIM),
        span_keys,
        preferred_element_type=jnp.float32,
    ) * HEAD_DIM ** (-0.5)
    key_pos = offset - WINDOW + jnp.arange(tok_rows + 2 * WINDOW, dtype=jnp.int32)
    total_len = tok_rows * lax.axis_size("ep")
    in_window = (
        (jnp.abs(positions[:, None] - key_pos[None, :]) <= WINDOW)
        & (key_pos[None, :] >= 0)
        & (key_pos[None, :] < total_len)
    )
    scores = jnp.where(in_window[None, None], scores, -1e30)
    sink_col = sink_logit.reshape(kv_local, group)[:, :, None]
    peak = jnp.maximum(jnp.max(scores, axis=-1), sink_col)[..., None]
    weights = jnp.exp(scores - peak)
    denominator = jnp.sum(weights, axis=-1, keepdims=True) + jnp.exp(sink_col[..., None] - peak)
    probs = (weights / denominator).astype(jnp.bfloat16)
    attended = jnp.einsum("hgqk,khd->qhgd", probs, span_values, preferred_element_type=jnp.float32)
    attended = attended.astype(jnp.bfloat16).reshape(tok_rows, heads_local * HEAD_DIM)
    rows_in = attended
    attend_out = lax.psum_scatter(
        jnp.dot(rows_in, w_output, preferred_element_type=jnp.float32).astype(jnp.bfloat16),
        "tp",
        scatter_dimension=0,
        tiled=True,
    )
    moe_rows = x_experts.shape[0]
    top_count = routes.shape[1]
    experts_n = lax.axis_size("ep")
    tp_count = lax.axis_size("tp")
    capacity = max(2, (3 * moe_rows * top_count + 2 * experts_n - 1) // (2 * experts_n))
    moe_normed = rms_scale(x_experts, expert_gain)
    flat_ids = routes.reshape(-1)
    onehot = (flat_ids[:, None] == jnp.arange(experts_n, dtype=jnp.int32)[None, :]).astype(
        jnp.int32
    )
    rank_in = jnp.cumsum(onehot, axis=0) - onehot
    slot_pos = jnp.sum(rank_in * onehot, axis=1)
    dest_slot = flat_ids * capacity + slot_pos
    owner_tok = jnp.arange(moe_rows * top_count, dtype=jnp.int32) // top_count
    slot_tok = jnp.full((experts_n * capacity,), moe_rows, jnp.int32).at[dest_slot].set(owner_tok)
    gate_mat = w_gate[0]
    up_mat = w_up[0]
    down_mat = w_down[0]
    col_width = model_width // tp_count
    own_cols = lax.dynamic_slice_in_dim(moe_normed, lax.axis_index("tp") * col_width, col_width, 1)
    padded_rows = jnp.concatenate([own_cols, jnp.zeros((1, col_width), jnp.bfloat16)], axis=0)
    outgoing = padded_rows[slot_tok].reshape(experts_n, capacity, col_width)
    arrived = lax.all_to_all(outgoing, "ep", split_axis=0, concat_axis=0, tiled=True)
    col_piece = collect(arrived, "tp", 2)
    rows_in = col_piece.reshape(experts_n * capacity, col_piece.shape[2])
    gate_act = jnp.dot(rows_in, gate_mat, preferred_element_type=jnp.float32)
    up_act = jnp.dot(rows_in, up_mat, preferred_element_type=jnp.float32)
    hidden = (jax.nn.silu(gate_act) * up_act).astype(jnp.bfloat16)
    partial_value = jnp.dot(hidden, down_mat, preferred_element_type=jnp.float32).astype(
        jnp.bfloat16
    )
    summed = (
        lax.psum_scatter(partial_value, "tp", scatter_dimension=1, tiled=True)
        .astype(jnp.float32)
        .astype(jnp.bfloat16)
    )
    summed = summed.reshape(experts_n, capacity, summed.shape[1])
    returned = lax.all_to_all(summed, "ep", split_axis=0, concat_axis=0, tiled=True)
    returned = returned.reshape(experts_n * capacity, returned.shape[2])
    picked = returned[dest_slot].astype(jnp.float32)
    route_weight = group_prob[:, None] * expert_prob / jnp.sum(expert_prob, axis=1, keepdims=True)
    expert_out = jnp.sum(
        picked.reshape(moe_rows, top_count, picked.shape[1]) * route_weight[:, :, None], axis=1
    )
    return (attend_out, expert_out.astype(jnp.bfloat16))


def solution(mesh):
    placed = (
        P("ep", None),
        P(),
        P(None, "tp"),
        P(None, "tp"),
        P(None, "tp"),
        P(),
        P(),
        P("tp"),
        P("tp", None),
        P("ep", None),
        P(),
        P("ep", None),
        P("ep"),
        P("ep", None),
        P("ep", None, "tp"),
        P("ep", None, "tp"),
        P("ep", "tp", None),
    )
    return jax.shard_map(
        per_device,
        mesh=mesh,
        in_specs=placed,
        out_specs=(P(("ep", "tp"), None), P("ep", "tp")),
        check_vma=False,
    )
```

profile of v0, /device:TPU:1, one launch (start us, length us, event | category | flops | bytes accessed | tf_op | source)
XLA Modules:
  0.0 275.5 jit_solution(4244649202895937723)
XLA Ops:
  7.2 3.6 %convert_element_type.89 = f32[384,2048]{1,0:T(8,128)} convert(bf16[384,2048]{1,0:T(8,128)(2,1)} %param.26) | non-fusion elementwise | flops 786432 | bytes 4718592 | tf_op jit(solution)/shard_map/convert_element_type | solution.py:44
  11.7 1.8 reduce-window.6
  14.3 3.4 %scatter_custom_fusion = s32[1152]{0:T(1024)S(1)} fusion(s32[768]{0:T(1024)S(1)} %fusion.41, s32[768]{0:T(1024)S(1)} %add_select_fusion, s32[]{:T(128)} %constant.107.clone.1), kind=kCustom, calls=%fused_computation.81 | custom fusion | bytes 4612 | tf_op jit(solution)/shard_map/scatter | solution.py:165
  18.5 1.3 fusion.22
  19.8 4.7 %gather_fusion = bf16[1152,512]{1,0:T(8,128)(2,1)} fusion(bf16[385,512]{1,0:T(8,128)(2,1)S(1)} %concatenate.36, s32[2048]{0:T(1024)S(1)} %pad_clamp_fusion), kind=kCustom, calls=%fused_computation | custom fusion | bytes 2363904 | tf_op jit(solution)/shard_map/gather | solution.py:172
  24.5 2.2 reshape.316
  26.7 51.8 %all_to_all.15 = bf16[64,18,512]{2,1,0:T(8,128)(2,1)S(1)} all-to-all(bf16[64,18,512]{2,1,0:T(8,128)(2,1)S(1)} %reshape.316), channel_id=1, replica_groups=mesh['ep'=64,'tp'=4] {'ep'}, dimensions={0} | all-to-all | bytes 2359296 | tf_op jit(solution)/shard_map/all_to_all | solution.py:173
  79.5 56.7 %all_to_all.16 = bf16[4,64,18,512]{3,1,2,0:T(8,128)(2,1)S(1)} all-to-all(bf16[4,64,18,512]{3,1,2,0:T(8,128)(2,1)S(1)} %broadcast_in_dim.18), channel_id=1, replica_groups=mesh['ep'=64,'tp'=4] {'tp'}, dimensions={0} | all-to-all | bytes 9437184 | tf_op jit(solution)/shard_map/all_to_all | solution.py:36
  136.2 3.6 %copy.52 = bf16[64,18,4,512]{3,2,1,0:T(4,128)(2,1)S(1)} copy(bf16[64,18,4,512]{3,0,1,2:T(8,128)(2,1)S(1)} %bitcast.78) | data formatting | bytes 9437184 | tf_op jit(solution)/shard_map/transpose | solution.py:31
  139.9 2.0 copy.58
  141.9 2.2 copy-done.3
  144.0 1.4 fusion.19
  145.5 9.3 %convolution_convert_fusion = bf16[1152,2048]{1,0:T(8,128)(2,1)} fusion(bf16[1152,2048]{1,0:T(8,128)(2,1)} %bitcast.81, f32[1152,256]{1,0:T(8,128)S(1)} %fusion.19, bf16[1,256,2048]{2,1,0:T(8,128)(2,1)S(1)} %copy-done, bf16[1,2048,256]{2,1,0:T(8,128)(2,1)S(1)} %copy-done.12), kind=kOutput, calls=%fused_computation.3 | convolution fusion | flops 2420047872 | bytes 12713984 | tf_op jit(solution)/shard_map/dot_general | solution.py:179
  155.5 0.9 copy-done.4
  156.9 2.0 multiply_reduce_fusion.3
  159.2 1.8 fusion.15
  161.0 5.0 %collective-permute-start = (bf16[2,128,128]{2,1,0:T(8,128)(2,1)S(1)}, bf16[2,128,128]{2,1,0:T(8,128)(2,1)S(1)}, u32[]{:S(2)}, u32[]{:S(2)}) collective-permute-start(bf16[2,128,128]{2,1,0:T(8,128)(2,1)S(1)} %get-tuple-element.8), channel_id=1, source_target_pairs={{0,4},{4,8},{8,12},{12,16},{16,20},{20,24},{24,28},{28,32},{32,36}... | collective-permute-start | bytes 196616 | tf_op jit(solution)/shard_map/ppermute | solution.py:22
  166.1 1.9 collective-permute-start.1
  168.1 2.2 multiply_reduce_fusion.2
  172.4 1.3 fusion.1
  173.8 1.4 fusion
  175.2 2.0 fusion.9
  177.2 2.1 convolution_convert_fusion.1
  179.4 26.2 %reduce-scatter.5.cloned.1.call-done = bf16[1152,512]{1,0:T(8,128)(2,1)} async-done(((bf16[1152,2048]{1,0:T(8,128)(2,1)}), bf16[1152,512]{1,0:T(8,128)(2,1)}) %reduce-scatter.5.cloned.1.call-update) | async-done | bytes 1179664 | tf_op jit(solution)/shard_map/reduce_scatter | solution.py:183
  205.6 3.0 %reshape.317 = bf16[64,18,512]{2,1,0:T(8,128)(2,1)} reshape(bf16[1152,512]{1,0:T(8,128)(2,1)} %reduce-scatter.5.cloned.1.call-done) | data formatting | bytes 2359296 | tf_op jit(solution)/shard_map/reshape | solution.py:187
  208.7 10.9 %all-to-all-start.2 = ((bf16[64,18,512]{2,1,0:T(8,128)(2,1)}), bf16[64,18,512]{2,1,0:T(8,128)(2,1)}, u32[]{:S(2)}, u32[]{:S(2)}) async-start(bf16[64,18,512]{2,1,0:T(8,128)(2,1)} %reshape.317), calls=%async_computation.4 | async-start | bytes 3145728 | tf_op jit(solution)/shard_map/all_to_all | solution.py:188
  219.6 0.8 copy.53
  220.5 38.1 %all-to-all-done.2 = bf16[64,18,512]{2,1,0:T(8,128)(2,1)} async-done(((bf16[64,18,512]{2,1,0:T(8,128)(2,1)}), bf16[64,18,512]{2,1,0:T(8,128)(2,1)}, u32[]{:S(2)}, u32[]{:S(2)}) %all-to-all-start.2) | async-done | bytes 1179680 | tf_op jit(solution)/shard_map/all_to_all | solution.py:188
  258.6 2.3 reshape.318
  260.9 2.7 gather_fusion.1
  263.5 1.0 reshape.319
  264.5 4.1 %multiply_reduce_fusion.1 = bf16[384,512]{1,0:T(8,128)(2,1)} fusion(f32[384,2,512]{2,1,0:T(2,128)S(1)} %reshape.319, f32[384,2]{1,0:T(8,128)} %copy.53), kind=kLoop, calls=%fused_computation.19 | loop fusion | flops 589824 | bytes 1969152 | tf_op jit(solution)/shard_map/reduce_sum | solution.py:192
  (84 shorter events, 7.2 us)
Async XLA Ops:
  7.2 138.3 %copy-start = (bf16[1,256,2048]{2,1,0:T(8,128)(2,1)S(1)}, bf16[1,256,2048]{2,1,0:T(8,128)(2,1)}, u32[]{:S(2)}) copy-start(bf16[1,256,2048]{2,1,0:T(8,128)(2,1)} %param.33) | copy-start | bytes 3145732
  7.2 3.7 %copy-start.2 = (bf16[384,2048]{1,0:T(8,128)(2,1)S(1)}, bf16[384,2048]{1,0:T(8,128)(2,1)}, u32[]{:S(2)}) copy-start(bf16[384,2048]{1,0:T(8,128)(2,1)} %param.26) | copy-start | bytes 4718596
  7.2 198.4 %reduce-scatter.5.cloned.1.call-start = ((), (), s32[]{:S(2)}) async-start(), calls=%async_computation.6 | async-start | bytes 5898240 | tf_op jit(solution)/shard_map/reduce_scatter | solution.py:183
  7.2 4.0 %copy-start.7 = (s32[384,2]{0,1:T(2,128)S(1)}, s32[384,2]{0,1:T(2,128)}, u32[]{:S(2)}) copy-start(s32[384,2]{0,1:T(2,128)} %param.28) | copy-start | bytes 9220
  139.9 4.2 %copy-start.11 = (bf16[1,2048,256]{2,1,0:T(8,128)(2,1)S(1)}, bf16[1,2048,256]{2,1,0:T(8,128)(2,1)}, u32[]{:S(2)}) copy-start(bf16[1,2048,256]{2,1,0:T(8,128)(2,1)} %param.31) | copy-start | bytes 3145732
  141.9 2.2 copy-start.3
  144.0 1.4 copy-start.12
  154.8 1.6 copy-start.4
  154.8 2.1 copy-start.13
  154.8 113.8 %reduce-scatter.3.cloned.1.call-start = ((), (), s32[]{:S(2)}) async-start(), calls=%async_computation.5 | async-start | bytes 2621440 | tf_op jit(solution)/shard_map/reduce_scatter | solution.py:145
  156.4 2.5 copy-start.9
  161.0 9.3 %copy-start.10 = (f32[64]{0:T(128)S(1)}, f32[64]{0:T(128)}, u32[]{:S(2)}) copy-start(f32[64]{0:T(128)} %param.22) | copy-start | bytes 772
  161.0 10.3 %collective-permute-start = (bf16[2,128,128]{2,1,0:T(8,128)(2,1)S(1)}, bf16[2,128,128]{2,1,0:T(8,128)(2,1)S(1)}, u32[]{:S(2)}, u32[]{:S(2)}) collective-permute-start(bf16[2,128,128]{2,1,0:T(8,128)(2,1)S(1)} %get-tuple-element.8), channel_id=1, source_target_pairs={{0,4},{4,8},{8,12},{12,16},{16,20},{20,24},{24,28},{28,32},{32,36}... | collective-permute-start | bytes 196616 | tf_op jit(solution)/shard_map/ppermute | solution.py:22
  166.1 6.0 %collective-permute-start.1 = (bf16[2,128,128]{2,1,0:T(8,128)(2,1)S(1)}, bf16[2,128,128]{2,1,0:T(8,128)(2,1)S(1)}, u32[]{:S(2)}, u32[]{:S(2)}) collective-permute-start(bf16[2,128,128]{2,1,0:T(8,128)(2,1)S(1)} %get-tuple-element.9), channel_id=1, source_target_pairs={{4,0},{8,4},{12,8},{16,12},{20,16},{24,20},{28,24},{32,28},{36,32}... | collective-permute-start | bytes 196616 | tf_op jit(solution)/shard_map/ppermute | solution.py:23
  168.0 3.2 %copy-start.14 = (f32[4]{0:T(128)S(1)}, f32[4]{0:T(128)}, u32[]{:S(2)}) copy-start(f32[4]{0:T(128)} %param.24) | copy-start | bytes 52
  175.2 2.0 copy-start.5
  179.4 40.2 %copy-start.6 = (f32[384,2]{0,1:T(2,128)S(1)}, f32[384,2]{0,1:T(2,128)}, u32[]{:S(2)}) copy-start(f32[384,2]{0,1:T(2,128)} %param.30) | copy-start | bytes 9220
  179.4 40.2 %copy-start.8 = (f32[384]{0:T(512)S(1)}, f32[384]{0:T(512)}, u32[]{:S(2)}) copy-start(f32[384]{0:T(512)} %param.29) | copy-start | bytes 4612
  208.7 49.9 %all-to-all-start.2 = ((bf16[64,18,512]{2,1,0:T(8,128)(2,1)}), bf16[64,18,512]{2,1,0:T(8,128)(2,1)}, u32[]{:S(2)}, u32[]{:S(2)}) async-start(bf16[64,18,512]{2,1,0:T(8,128)(2,1)} %reshape.317), calls=%async_computation.4 | async-start | bytes 3145728 | tf_op jit(solution)/shard_map/all_to_all | solution.py:188
  260.8 7.8 %copy-start.1 = (bf16[1,256,2048]{2,1,0:T(8,128)(2,1)S(1)}, bf16[1,256,2048]{2,1,0:T(8,128)(2,1)}, u32[]{:S(2)}) copy-start(bf16[1,256,2048]{2,1,0:T(8,128)(2,1)} %param.33) | copy-start | bytes 3145732
Sparse Core Ops, SparseCore 0:
  155.0 50.6 reduce-scatter.4
  208.8 32.0 reduce-scatter.2
where the time goes:
time: 276 us; the launch traced here: 275 us
  blocking collectives  109 us (39%)
  waiting for transfers between devices  65.1 us (24%)
  local copies, waits for them, and re-layouts  32.1 us (12%)
  matrix products  22.1 us (8%)
  starting transfers between devices  18.2 us (7%)
  other arithmetic  14.9 us (5%)
  between operations  14.6 us (5%)
    all_to_all x1, blocking collectives, sent_to_all(): return lax.all_to_all(copies, axis, split_axis=0, concat_axis=0, tiled=True)  56.7 us
    all_to_all x1, blocking collectives, per_device(): lax.all_to_all(outgoing, 'ep', split_axis=0, concat_axis=0, tiled=True)  51.8 us
    all_to_all x1, waiting for transfers between devices, per_device(): lax.all_to_all(summed, 'ep', split_axis=0, concat_axis=0, tiled=True)  38.1 us
    reduce_scatter x1, waiting for transfers between devices, per_device(): lax.psum_scatter(partial_value, 'tp', scatter_dimension=1, tiled=True)  26.2 us
    all_to_all x1, starting transfers between devices, per_device(): lax.all_to_all(summed, 'ep', split_axis=0, concat_axis=0, tiled=True)  10.9 us
    dot_general x1, matrix products, per_device(): jnp.dot(hidden, down_mat, preferred_element_type=jnp.float32)  9.33 us
  transfers between devices with their start and end apart: 5, of which 3 were waited for; matrix products, arithmetic and copies ran while one was open for 11% of the time, Pallas kernels for 0%

commit v1 on v0

v1 whole, which is shorter than its diff:
```python
import functools

import jax
import jax.numpy as jnp
import numpy as np
from jax import lax
from jax.experimental import pallas as pl
from jax.experimental.pallas import tpu as pltpu
from jax.sharding import PartitionSpec as P

HEAD_DIM = 64
WINDOW = 128
GRID_W = 64
MAIN = 16
EXTRA = 2

epsilon = 1e-06
rope_base = 10000.0

BF = jnp.bfloat16
F32 = jnp.float32
MESH = pl.DeviceIdType.MESH


def dot(a, b):
    return jnp.dot(a, b, preferred_element_type=F32)


def iota(shape, dim):
    return lax.broadcasted_iota(jnp.int32, shape, dim)


def kernel(dims, *refs):
    nz, npl, n_tp, tok_m, tok_a, width, ff, qw, kw = dims
    (
        routes_ref, routes_t_ref, weight_ref, egain_ref, again_ref, consts_ref, sink_ref,
        xm_hbm, wg_hbm, wu_hbm, wd_hbm, xa_hbm, wq_hbm, wk_hbm, wv_hbm, wo_hbm,
        attend_ref, expert_ref,
        xm, wg, wu, wd, xa, wqkv, wo,
        own, out_main, out_ext, grid_in, ext_in, part, rb1, sb, rb2, res_main, res_ext, back_main,
        back_ext, acc, normed, qs, kv, att, opart, ra1, sa, ra2,
        load_sem, disp_s, disp_r, ret_s, ret_r, ag_s, ag_r, rs_s, rs_r, halo_s, halo_r, ar_s, ar_r,
    ) = refs
    qd = width // n_tp
    half = qd // 2
    main_rows, ext_rows = npl * MAIN, npl * EXTRA
    chunk = main_rows + ext_rows
    eb = EXTRA * qd // 128
    n_ep = nz * npl
    ep = lax.axis_index("ep")
    tp = lax.axis_index("tp")
    z = ep // npl
    p = ep % npl
    right, left, opp = (tp + 1) % n_tp, (tp + n_tp - 1) % n_tp, (tp + 2) % n_tp
    after, before = (ep + 1) % n_ep, (ep + n_ep - 1) % n_ep

    barrier = pltpu.get_barrier_semaphore()

    def greet(k, carry):
        pl.semaphore_signal(barrier, inc=1, device_id={"ep": (ep + k) % n_ep}, device_id_type=MESH)
        return carry

    lax.fori_loop(1, n_ep, greet, 0)
    for side in (left, right):
        pl.semaphore_signal(barrier, inc=1, device_id={"tp": side}, device_id_type=MESH)

    loads = [
        (xm_hbm, xm), (xa_hbm, xa), (wq_hbm, wqkv.at[:, 0:qw]), (wk_hbm, wqkv.at[:, qw:qw + kw]),
        (wv_hbm, wqkv.at[:, qw + kw:qw + 2 * kw]), (wo_hbm, wo),
        (wg_hbm.at[0], wg), (wu_hbm.at[0], wu), (wd_hbm.at[0], wd),
    ]
    loads = [pltpu.make_async_copy(s, d, load_sem.at[i]) for i, (s, d) in enumerate(loads)]
    for copy in loads:
        copy.start()

    def slots(ids, axis):
        shape = (tok_m, n_ep) if axis == 0 else (n_ep, tok_m)
        experts = iota(shape, 1 - axis)
        hots = [(experts == r) for r in ids]
        lower = iota((tok_m, tok_m), 1 - axis) < iota((tok_m, tok_m), axis)
        tri = jnp.where(lower, 1.0, 0.0).astype(BF)
        result = []
        base = None
        for hot, r in zip(hots, ids):
            hot_b = jnp.where(hot, 1.0, 0.0).astype(BF)
            ranks = dot(tri, hot_b) if axis == 0 else dot(hot_b, tri)
            if base is not None:
                ranks = ranks + base
            else:
                base = jnp.sum(hot_b.astype(F32), axis=axis, keepdims=True)
            rank = jnp.sum(jnp.where(hot, ranks, 0.0), axis=1 - axis, keepdims=True).astype(jnp.int32)
            dz = lax.rem((r // npl) - z + nz, nz)
            index = jnp.where(2 * dz <= nz, jnp.maximum(2 * dz - 1, 0), 2 * (nz - dz))
            place = lax.rem(r, npl)
            inside = jnp.where(rank < MAIN, place * MAIN + rank, main_rows + place * EXTRA + rank - MAIN)
            result.append(index * chunk + inside)
        return result

    rows_t = routes_t_ref[...]
    slot_row = slots([rows_t[0:1, :], rows_t[1:2, :]], 1)
    rows_c = routes_ref[...]
    slot_col = slots([rows_c[:, 0:1], rows_c[:, 1:2]], 0)

    loads[0].wait()
    col0 = pl.multiple_of(tp * qd, 128)

    def norm_m(b, carry):
        rows = pl.ds(pl.multiple_of(b * 32, 32), 32)
        v = xm[rows, :].astype(F32)
        scale = lax.rsqrt(jnp.mean(v * v, axis=-1, keepdims=True) + epsilon)
        mine = xm[rows, pl.ds(col0, qd)].astype(F32)
        own[rows, :] = (mine * scale * egain_ref[:, pl.ds(col0, qd)]).astype(BF)
        return carry

    lax.fori_loop(0, tok_m // 32, norm_m, 0)
    pl.semaphore_wait(barrier, n_ep - 1 + 2)

    def delta(i):
        odd = lax.rem(i, 2)
        return odd * ((i + 1) // 2) - (1 - odd) * (i // 2)

    def fold_ext(e):
        total = jnp.zeros((npl * eb, 128), F32)
        r = iota((npl * eb, ext_rows), 0)
        c = iota((npl * eb, ext_rows), 1)
        src = (r // eb) * EXTRA + lax.rem(r, eb) // (qd // 128)
        for j in range(qd // 128):
            pick = jnp.where((src == c) & (lax.rem(r, qd // 128) == j), 1.0, 0.0).astype(BF)
            total = total + dot(pick, e[:, j * 128:(j + 1) * 128])
        return total.reshape(npl, eb, 128).astype(BF)

    def unfold_ext(x):
        flat = x.astype(F32).reshape(npl * eb, 128).astype(BF)
        r = iota((ext_rows, npl * eb), 0)
        c = iota((ext_rows, npl * eb), 1)
        want = (r // EXTRA) * eb + lax.rem(r, EXTRA) * (qd // 128)
        out = []
        for j in range(qd // 128):
            pick = jnp.where(want + j == c, 1.0, 0.0).astype(BF)
            out.append(dot(pick, flat).astype(BF))
        return out

    def exchange(i, main, ext, land_main, land_ext, sems, recv, dest_z):
        def body(k, carry):
            q = lax.rem(p + k, npl)
            dev = {"ep": dest_z * npl + q}
            pltpu.make_async_remote_copy(
                src_ref=main.at[i, pl.ds(pl.multiple_of(q * MAIN, MAIN), MAIN), :],
                dst_ref=land_main, send_sem=sems.at[i, 0], recv_sem=recv.at[i, 0],
                device_id=dev, device_id_type=MESH,
            ).start()
            pltpu.make_async_remote_copy(
                src_ref=ext.at[i, q], dst_ref=land_ext, send_sem=sems.at[i, 1],
                recv_sem=recv.at[i, 1], device_id=dev, device_id_type=MESH,
            ).start()
            return carry

        lax.fori_loop(1 - jnp.minimum(i, 1), npl, body, 0)

    def settle(i, main, ext, sems):
        for j, ref in ((0, main), (1, ext)):
            full = ref.at[i]
            few = ref.at[i, 0:(npl - 1) * MAIN, :] if j == 0 else ref.at[i, 0:npl - 1]

            @pl.when(i > 0)
            def _():
                pltpu.make_async_copy(full, full, sems.at[i, j]).wait()

            @pl.when(i == 0)
            def _():
                pltpu.make_async_copy(few, few, sems.at[i, j]).wait()

    my_main = pl.ds(pl.multiple_of(p * MAIN, MAIN), MAIN)
    my_cols = pl.ds(col0, qd)

    def dispatch(i, carry):
        slot = iota((chunk, tok_m), 0) + i * chunk
        hot = jnp.where((slot == slot_row[0]) | (slot == slot_row[1]), 1.0, 0.0).astype(BF)
        rows = dot(hot, own[...]).astype(BF)
        out_main[i] = rows[0:main_rows]
        out_ext[i] = fold_ext(rows[main_rows:])
        exchange(
            i, out_main, out_ext, grid_in.at[i, my_main, my_cols], ext_in.at[i, p],
            disp_s, disp_r, lax.rem(z + delta(i) + nz, nz),
        )
        return carry

    lax.fori_loop(0, nz, dispatch, 0)
    grid_in[0, my_main, my_cols] = out_main[0, my_main, :]
    ext_in[0, p] = out_ext[0, p]
    acc[...] = jnp.zeros_like(acc)

    def remote(src, dst, sems, recv, dev):
        return pltpu.make_async_remote_copy(
            src_ref=src, dst_ref=dst, send_sem=sems, recv_sem=recv, device_id={"tp": dev},
            device_id_type=MESH,
        )

    def cols(quarter, off, size):
        return pl.ds(pl.multiple_of(quarter * qd + off, 128), size)

    def ag_own(i):
        block = grid_in.at[i, :, my_cols]
        return [remote(block, block, ag_s.at[i, s], ag_r.at[i, s], d) for s, d in ((0, right), (1, left))]

    def ag_fwd(i):
        a = grid_in.at[i, :, cols(left, 0, half)]
        b = grid_in.at[i, :, cols(right, half, half)]
        return [
            remote(a, a, ag_s.at[i, 2], ag_r.at[i, 2], right),
            remote(b, b, ag_s.at[i, 3], ag_r.at[i, 3], left),
        ]

    def rs_one(i):
        return [
            remote(part.at[i, :, cols(opp, 0, half)], rb1.at[i, 0], rs_s.at[i, 0], rs_r.at[i, 0], right),
            remote(part.at[i, :, cols(opp, half, half)], rb1.at[i, 1], rs_s.at[i, 1], rs_r.at[i, 1], left),
        ]

    def rs_side(i):
        return [
            remote(part.at[i, :, cols(right, half, half)], rb2.at[i, 0, :, half:qd], rs_s.at[i, 2],
                   rs_r.at[i, 2], right),
            remote(part.at[i, :, cols(left, 0, half)], rb2.at[i, 1, :, 0:half], rs_s.at[i, 3],
                   rs_r.at[i, 3], left),
        ]

    def rs_two(i):
        return [
            remote(sb.at[i, 0], rb2.at[i, 0, :, 0:half], rs_s.at[i, 4], rs_r.at[i, 4], right),
            remote(sb.at[i, 1], rb2.at[i, 1, :, half:qd], rs_s.at[i, 5], rs_r.at[i, 5], left),
        ]

    quarter_rows = tok_a // n_tp
    hw = width // 2

    def rows_of(t):
        return pl.ds(pl.multiple_of(t * quarter_rows, quarter_rows), quarter_rows)

    def ar_one():
        return [
            remote(opart.at[rows_of(opp), 0:hw], ra1.at[0], ar_s.at[0], ar_r.at[0], right),
            remote(opart.at[rows_of(opp), hw:width], ra1.at[1], ar_s.at[1], ar_r.at[1], left),
        ]

    def ar_side():
        return [
            remote(opart.at[rows_of(right), hw:width], ra2.at[0, :, hw:width], ar_s.at[2], ar_r.at[2], right),
            remote(opart.at[rows_of(left), 0:hw], ra2.at[1, :, 0:hw], ar_s.at[3], ar_r.at[3], left),
        ]

    def ar_two():
        return [
            remote(sa.at[0], ra2.at[0, :, 0:hw], ar_s.at[4], ar_r.at[4], right),
            remote(sa.at[1], ra2.at[1, :, hw:width], ar_s.at[5], ar_r.at[5], left),
        ]

    def halo():
        out = []
        for s, (dev, src, dst) in enumerate((
            (after, kv.at[tok_a:tok_a + WINDOW, :], kv.at[0:WINDOW, :]),
            (before, kv.at[WINDOW:2 * WINDOW, :], kv.at[tok_a + WINDOW:tok_a + 2 * WINDOW, :]),
        )):
            out.append(pltpu.make_async_remote_copy(
                src_ref=src, dst_ref=dst, send_sem=halo_s.at[s], recv_sem=halo_r.at[s],
                device_id={"ep": dev}, device_id_type=MESH,
            ))
        return out

    def start(copies):
        for c in copies:
            c.start()

    def arrived(copies):
        for c in copies:
            c.wait_recv()

    def sent(copies):
        for c in copies:
            c.wait_send()

    half_dim = HEAD_DIM // 2

    def qkv_all():
        for copy in loads[1:5]:
            copy.wait()
        inv = consts_ref[2:3, :]
        lane = lax.rem(iota((GRID_W, 128), 1), half_dim)
        is_row = lane < half_dim // 2
        col_ang = iota((GRID_W, 128), 0).astype(F32) * inv
        groups = tok_a // GRID_W
        row_ang = (iota((groups, 128), 0) + ep * groups).astype(F32) * inv
        col_cos, col_sin = jnp.cos(col_ang), jnp.sin(col_ang)
        row_cos, row_sin = jnp.cos(row_ang), jnp.sin(row_ang)
        first = lax.rem(iota((1, 128), 1), HEAD_DIM) < half_dim
        sign = jnp.where(first, -1.0, 1.0)
        tables = []
        for g in range(groups):
            c = jnp.where(is_row, row_cos[g:g + 1, :], col_cos)
            s = jnp.where(is_row, row_sin[g:g + 1, :], col_sin) * sign
            tables.append((c, s))
        ones = jnp.where(iota((128, 128), 0) // HEAD_DIM == iota((128, 128), 1) // HEAD_DIM, 1.0, 0.0).astype(BF)

        def rotated(v, gain, c, s):
            sq = v * v
            hi = sq.astype(BF)
            lo = (sq - hi.astype(F32)).astype(BF)
            mean = (dot(hi, ones) + dot(lo, ones)) * (1.0 / HEAD_DIM)
            scaled = v * lax.rsqrt(mean + epsilon) * gain
            other = jnp.where(first, pltpu.roll(scaled, 128 - half_dim, 1), pltpu.roll(scaled, half_dim, 1))
            return (scaled * c + other * s).astype(BF)

        blk = 128
        for b in range(tok_a // blk):
            def norm_a(j, carry):
                rows = pl.ds(pl.multiple_of(b * blk + j * 32, 32), 32)
                v = xa[rows, :].astype(F32)
                scale = lax.rsqrt(jnp.mean(v * v, axis=-1, keepdims=True) + epsilon)
                normed[rows, :] = (v * scale * again_ref[...]).astype(BF)
                return carry

            lax.fori_loop(0, blk // 32, norm_a, 0)
            rows = slice(b * blk, (b + 1) * blk)
            proj = dot(normed[rows, :], wqkv[...])
            per = blk // GRID_W
            c = jnp.concatenate([tables[b * per + j][0] for j in range(per)], axis=0)
            s = jnp.concatenate([tables[b * per + j][1] for j in range(per)], axis=0)
            for j in range(qw // 128):
                sl = slice(j * 128, (j + 1) * 128)
                qs[rows, sl] = rotated(proj[:, sl], consts_ref[0:1, :], c, s)
            dst = slice(WINDOW + b * blk, WINDOW + (b + 1) * blk)
            kv[dst, 0:kw] = rotated(proj[:, qw:qw + kw], consts_ref[1:2, :], c, s)
            kv[dst, kw:2 * kw] = proj[:, qw + kw:qw + 2 * kw].astype(BF)

    kv_local = kw // HEAD_DIM
    group = qw // kw

    def attend_all():
        loads[5].wait()
        total_len = tok_a * n_ep
        span = 3 * WINDOW

        def block(b, carry):
            row0 = pl.multiple_of(b * WINDOW, WINDOW)
            q_rows = pl.ds(row0, WINDOW)
            k_rows = pl.ds(row0, span)
            gap = iota((WINDOW, span), 1) - iota((WINDOW, span), 0)
            pos = ep * tok_a - WINDOW + row0 + iota((WINDOW, span), 1)
            valid = (gap >= 0) & (gap <= 2 * WINDOW) & (pos >= 0) & (pos < total_len)
            for h in range(kv_local):
                keys = kv[k_rows, h * HEAD_DIM:(h + 1) * HEAD_DIM]
                vals = kv[k_rows, kw + h * HEAD_DIM:kw + (h + 1) * HEAD_DIM]
                for g in range(group):
                    head = h * group + g
                    lanes = slice(head * HEAD_DIM, (head + 1) * HEAD_DIM)
                    q = qs[q_rows, lanes]
                    s = lax.dot_general(q, keys, (((1,), (1,)), ((), ())), preferred_element_type=F32)
                    s = jnp.where(valid, s * HEAD_DIM ** (-0.5), -1e30)
                    sink = sink_ref[head]
                    peak = jnp.maximum(jnp.max(s, axis=-1, keepdims=True), sink)
                    w = jnp.exp(s - peak)
                    denom = jnp.sum(w, axis=-1, keepdims=True) + jnp.exp(sink - peak)
                    probs = (w * (1.0 / denom)).astype(BF)
                    att[:, lanes] = dot(probs, vals).astype(BF)
            opart[q_rows, :] = dot(att[...], wo[...]).astype(BF)
            return carry

        lax.fori_loop(0, tok_a // WINDOW, block, 0)

    def tick(i, carry):
        @pl.when(i < nz)
        def _():
            settle(i, out_main, ext_in, disp_r)
            e = unfold_ext(ext_in[i])
            for j, piece in enumerate(e):
                grid_in[i, main_rows:chunk, cols(tp, j * 128, 128)] = piece
            start(ag_own(i))

        @pl.when((i >= 1) & (i < nz + 1))
        def _():
            arrived(ag_own(i - 1))
            start(ag_fwd(i - 1))

        @pl.when(i == 0)
        def _():
            qkv_all()
            start(halo())

        @pl.when((i >= 2) & (i < nz + 2))
        def _():
            c = i - 2

            @pl.when(c == 0)
            def _():
                for copy in loads[6:9]:
                    copy.wait()

            arrived(ag_fwd(c))
            x = grid_in[c]
            g = dot(x, wg[...])
            u = dot(x, wu[...])
            hidden = (g / (1.0 + jnp.exp(-g)) * u).astype(BF)
            part[c] = dot(hidden, wd[...]).astype(BF)
            start(rs_one(c))
            start(rs_side(c))

        @pl.when((i >= 3) & (i < nz + 3))
        def _():
            c = i - 3
            arrived(rs_one(c))
            for s, (quarter, off) in enumerate(((right, 0), (left, half))):
                mine = part[c, :, cols(quarter, off, half)].astype(F32)
                sb[c, s] = (mine + rb1[c, s].astype(F32)).astype(BF)
            start(rs_two(c))

        @pl.when((i >= 4) & (i < nz + 4))
        def _():
            c = i - 4
            arrived(rs_side(c))
            arrived(rs_two(c))
            total = part[c, :, my_cols].astype(F32) + rb2[c, 0].astype(F32) + rb2[c, 1].astype(F32)
            total = total.astype(BF)
            res_main[c] = total[0:main_rows]
            res_ext[c] = fold_ext(total[main_rows:])
            exchange(
                c, res_main, res_ext, back_main.at[c, my_main, :], back_ext.at[c, p],
                ret_s, ret_r, lax.rem(z - delta(c) + nz, nz),
            )

            @pl.when(c == 0)
            def _():
                back_main[0, my_main, :] = res_main[0, my_main, :]
                back_ext[0, p] = res_ext[0, p]

        @pl.when(i == 1)
        def _():
            arrived(halo())
            attend_all()
            start(ar_one())
            start(ar_side())

        @pl.when(i == 2)
        def _():
            arrived(ar_one())
            for s, (t, off) in enumerate(((right, 0), (left, hw))):
                mine = opart[rows_of(t), off:off + hw].astype(F32)
                sa[s] = (mine + ra1[s].astype(F32)).astype(BF)
            start(ar_two())

        @pl.when(i == 4)
        def _():
            arrived(ar_side())
            arrived(ar_two())
            total = opart[rows_of(tp), :].astype(F32) + ra2[0].astype(F32) + ra2[1].astype(F32)
            attend_ref[...] = total.astype(BF)

        @pl.when(i >= 5)
        def _():
            c = i - 5
            settle(c, back_main, back_ext, ret_r)
            e = unfold_ext(back_ext[c])
            slot = iota((tok_m, chunk), 1) + c * chunk
            for k in range(2):
                hot = jnp.where(slot == slot_col[k], 1.0, 0.0).astype(BF)
                acc[k] += dot(hot[:, 0:main_rows], back_main[c])
                for j, piece in enumerate(e):
                    sl = slice(j * 128, (j + 1) * 128)
                    acc[k, :, sl] += dot(hot[:, main_rows:], piece)

        return carry

    lax.fori_loop(0, nz + 5, tick, 0)
    weights = weight_ref[...]
    expert_ref[...] = (acc[0] * weights[:, 0:1] + acc[1] * weights[:, 1:2]).astype(BF)

    def drain(i, carry):
        settle(i, out_main, out_ext, disp_s)
        settle(i, res_main, res_ext, ret_s)
        for stage in (ag_own, ag_fwd, rs_one, rs_side, rs_two):
            sent(stage(i))
        return carry

    lax.fori_loop(0, nz, drain, 0)
    for stage in (halo, ar_one, ar_side, ar_two):
        sent(stage())


def fused(dims, *args):
    nz, npl, n_tp, tok_m, tok_a, width, ff, qw, kw = dims
    qd = width // n_tp
    half = qd // 2
    chunk = npl * (MAIN + EXTRA)
    eb = EXTRA * qd // 128
    hw = width // 2
    qr = tok_a // n_tp
    vm = pltpu.VMEM
    dma = pltpu.SemaphoreType.DMA
    any_spec = pl.BlockSpec(memory_space=pl.ANY)
    vmem_spec = pl.BlockSpec(memory_space=pltpu.VMEM)
    smem_spec = pl.BlockSpec(memory_space=pltpu.SMEM)
    return pl.pallas_call(
        functools.partial(kernel, dims),
        out_shape=(
            jax.ShapeDtypeStruct((qr, width), BF),
            jax.ShapeDtypeStruct((tok_m, qd), BF),
        ),
        in_specs=[vmem_spec] * 6 + [smem_spec] + [any_spec] * 9,
        out_specs=(vmem_spec, vmem_spec),
        scratch_shapes=[
            vm((tok_m, width), BF), vm((width, ff), BF), vm((width, ff), BF), vm((ff, width), BF),
            vm((tok_a, width), BF), vm((width, qw + 2 * kw), BF), vm((qw, width), BF),
            vm((tok_m, qd), BF),
            vm((nz, npl * MAIN, qd), BF), vm((nz, npl, eb, 128), BF),
            vm((nz, chunk, width), BF), vm((nz, npl, eb, 128), BF),
            vm((nz, chunk, width), BF),
            vm((nz, 2, chunk, half), BF), vm((nz, 2, chunk, half), BF), vm((nz, 2, chunk, qd), BF),
            vm((nz, npl * MAIN, qd), BF), vm((nz, npl, eb, 128), BF),
            vm((nz, npl * MAIN, qd), BF), vm((nz, npl, eb, 128), BF),
            vm((2, tok_m, qd), F32),
            vm((tok_a, width), BF), vm((tok_a, qw), BF), vm((tok_a + 2 * WINDOW, 2 * kw), BF),
            vm((WINDOW, qw), BF), vm((tok_a, width), BF),
            vm((2, qr, hw), BF), vm((2, qr, hw), BF), vm((2, qr, width), BF),
            dma((9,)), dma((nz, 2)), dma((nz, 2)), dma((nz, 2)), dma((nz, 2)),
            dma((nz, 4)), dma((nz, 4)), dma((nz, 6)), dma((nz, 6)),
            dma((2,)), dma((2,)), dma((6,)), dma((6,)),
        ],
        compiler_params=pltpu.CompilerParams(
            collective_id=0, has_side_effects=True, vmem_limit_bytes=60 * 1024 * 1024
        ),
        name="fused_layer",
    )(*args)


def per_device(
    planes,
    x_attend, attend_gain, w_query, w_key, w_value, query_gain, key_gain, sink_logit, w_output,
    x_experts, expert_gain, routes, group_prob, expert_prob, w_gate, w_up, w_down,
):
    n_ep, n_tp = lax.axis_size("ep"), lax.axis_size("tp")
    tok_a, width = x_attend.shape
    dims = (
        planes, n_ep // planes, n_tp, x_experts.shape[0], tok_a, width, w_gate.shape[2],
        w_query.shape[1], w_key.shape[1],
    )
    half_dim = HEAD_DIM // 2
    inverse = rope_base ** (-jnp.arange(0, half_dim, 2, dtype=jnp.float32) / half_dim)
    consts = jnp.stack([
        jnp.tile(query_gain, 2), jnp.tile(key_gain, 2), jnp.tile(inverse, 256 // half_dim),
    ])
    weights = group_prob[:, None] * expert_prob / jnp.sum(expert_prob, axis=1, keepdims=True)
    return fused(
        dims, routes, routes.T, weights, expert_gain[None, :], attend_gain[None, :], consts,
        sink_logit, x_experts, w_gate, w_up, w_down, x_attend, w_query, w_key, w_value, w_output,
    )


def solution(mesh, planes=8):
    placed = (
        P("ep", None), P(), P(None, "tp"), P(None, "tp"), P(None, "tp"), P(), P(), P("tp"),
        P("tp", None), P("ep", None), P(), P("ep", None), P("ep"), P("ep", None),
        P("ep", None, "tp"), P("ep", None, "tp"), P("ep", "tp", None),
    )
    return jax.shard_map(
        functools.partial(per_device, planes),
        mesh=mesh,
        in_specs=placed,
        out_specs=(P(("ep", "tp"), None), P("ep", "tp")),
        check_vma=False,
    )
```

time: 276 us -> 158 us (0.57)
  Pallas kernels: 0 us -> 149 us
  blocking collectives: 109 us -> 0 us
  waiting for transfers between devices: 65.1 us -> 0 us
  local copies, waits for them, and re-layouts: 32.1 us -> 6.85 us
  matrix products: 22.1 us -> 0 us
  starting transfers between devices: 18.2 us -> 0 us
  between operations: 14.6 us -> 0.65 us
  other arithmetic: 14.9 us -> 2.14 us
    pallas_call x0 -> x1, Pallas kernels: none -> 149 us  [fused(): pl.pallas_call(functools.partial(kernel, dims), out_shape=(jax.ShapeDtype...]
    all_to_all x2 -> x0, blocking collectives: 109 us -> none  [the longest x1 56.7 us: sent_to_all(): return lax.all_to_all(copies, axis, split_axis=0, concat_axis=0, tiled=True)]
    all_to_all x1 -> x0, waiting for transfers between devices: 38.1 us -> none  [per_device(): lax.all_to_all(summed, 'ep', split_axis=0, concat_axis=0, tiled=True)]
    reduce_scatter x2 -> x0, waiting for transfers between devices: 26.2 us -> none  [the longest x1 26.2 us: per_device(): lax.psum_scatter(partial_value, 'tp', scatter_dimension=1, tiled=True)]
    dot_general x8 -> x0, matrix products: 22.1 us -> none  [the longest x1 9.33 us: per_device(): jnp.dot(hidden, down_mat, preferred_element_type=jnp.float32)]
    all_to_all x1 -> x0, starting transfers between devices: 10.9 us -> none  [per_device(): lax.all_to_all(summed, 'ep', split_axis=0, concat_axis=0, tiled=True)]
    reshape x3 -> x0, local copies, waits for them, and re-layouts: 7.48 us -> none  [the longest x1 3.03 us: per_device(): summed = summed.reshape(experts_n, capacity, summed.shape[1])]
    gather x2 -> x0, local copies, waits for them, and re-layouts: 7.35 us -> none  [the longest x1 4.67 us: per_device(): outgoing = padded_rows[slot_tok].reshape(experts_n, capacity, col_width)]
  transfers between devices with their start and end apart: 5 -> 0, of which waited for: 3 -> 0; matrix products, arithmetic and copies ran while one was open for 11% -> 0% of each run, Pallas kernels for 0% -> 0%
where the time goes in v1:
time: 158 us
  Pallas kernels  149 us (94%)
  local copies, waits for them, and re-layouts  6.85 us (4%)
  other arithmetic  2.14 us (1%)
    pallas_call x1, Pallas kernels, fused(): pl.pallas_call(functools.partial(kernel, dims), out_shape=(jax.ShapeDtype...  149 us
    unnamed x3, local copies, waits for them, and re-layouts  5.15 us

profile of v1, /device:TPU:1, one launch (start us, length us, event | category | flops | bytes accessed | tf_op | source)
XLA Modules:
  0.0 158.2 jit_solution(8220230621437658436)
XLA Ops:
  0.6 0.7 tile.6
  1.3 0.1 stack_tile.9
  1.4 0.7 tile.7
  2.0 0.1 stack_tile.10
  2.1 0.1 stack_tile.11
  2.2 0.6 pad_maximum_fusion.refs_5_
  2.8 0.7 fusion
  3.5 0.1 copy.22
  3.7 0.8 broadcast_divide_fusion.refs_2_
  4.5 1.5 copy.24.refs_0_
  6.0 148.5 %fused_layer.1 = (bf16[128,2048]{1,0:T(8,128)(2,1)}, bf16[384,512]{1,0:T(8,128)(2,1)}) custom-call(s32[384,2]{1,0:T(8,128)} %copy.24.refs_0_, s32[2,384]{1,0:T(2,128)} %bitcast.3, f32[384,2]{1,0:T(8,128)} %broadcast_divide_fusion.refs_2_, f32[1,2048]{1,0:T(1,128)} %bitcast.4, f32[1,2048]{1,0:T(1,128)} %bitcast.5, f32[3,128]{1,0:T(4,128)} %pad_maximum_fusion.refs_5_, ...), custom_call_target="tpu_custom_call" | custom-call | tf_op jit(solution)/shard_map/fused_layer/pallas_call | solution.py:501
  154.5 1.9 %copy.27 = bf16[128,2048]{1,0:T(8,128)(2,1)} copy(bf16[128,2048]{1,0:T(8,128)(2,1)} %get-tuple-element.6) | data formatting | bytes 1048576
  156.4 1.8 %copy.28 = bf16[384,512]{1,0:T(8,128)(2,1)} copy(bf16[384,512]{1,0:T(8,128)(2,1)} %get-tuple-element.7) | data formatting | bytes 786432
  (2 shorter events, 0.0 us)

commit v2 on v1

v2 whole, which is shorter than its diff:
```python
import functools

import jax
import jax.numpy as jnp
import numpy as np
from jax import lax
from jax.experimental import pallas as pl
from jax.experimental.pallas import tpu as pltpu
from jax.sharding import PartitionSpec as P

HEAD_DIM = 64
WINDOW = 128
GRID_W = 64
MAIN = 16
EXTRA = 2
FIRST_ATT = 3
LAG = 4

epsilon = 1e-06
rope_base = 10000.0

BF = jnp.bfloat16
F32 = jnp.float32
MESH = pl.DeviceIdType.MESH


def dot(a, b):
    return jnp.dot(a, b, preferred_element_type=F32)


def iota(shape, dim):
    return lax.broadcasted_iota(jnp.int32, shape, dim)


ORDERS = {8: ((0, 2, 6, 5, 4, 3, 7, 1), 5), 4: ((0, 2, 3, 1), 1), 2: ((0, 1), 1)}


def kernel(dims, *refs):
    nz, npl, n_tp, tok_m, tok_a, width, ff, qw, kw = dims
    (
        routes_ref, prob_ref, gprob_ref, egain_ref, again_ref, qgain_ref, kgain_ref, inv_ref, sink_ref,
        xm_hbm, wg_hbm, wu_hbm, wd_hbm, xa_hbm, wq_hbm, wk_hbm, wv_hbm, wo_hbm,
        attend_ref, expert_ref,
        xm, wg, wu, wd, xa, wqkv, wo,
        own, out_main, out_ext, full_main, full_ext, grid_in, ext_in, fext_in, part, rb1, sb, rb2,
        res_main, res_ext, back_main, back_ext, acc, normed, qs, kv, att, att_all,
        load_sem, disp_s, disp_r, ret_s, ret_r, ag_s, ag_r, rs_s, rs_r, halo_s, halo_r, wo_s, wo_r, at_s, at_r,
    ) = refs
    order, n_ag = ORDERS[nz]
    qd = width // n_tp
    half = qd // 2
    main_rows, ext_rows = npl * MAIN, npl * EXTRA
    chunk = main_rows + ext_rows
    eb = EXTRA * qd // 128
    n_ep = nz * npl
    ep = lax.axis_index("ep")
    tp = lax.axis_index("tp")
    z = ep // npl
    p = ep % npl
    nx = npl // 2
    xc, core = p // 2, p % 2
    right, left, opp = (tp + 1) % n_tp, (tp + n_tp - 1) % n_tp, (tp + 2) % n_tp
    after, before = (ep + 1) % n_ep, (ep + n_ep - 1) % n_ep

    barrier = pltpu.get_barrier_semaphore()

    def greet(k, carry):
        pl.semaphore_signal(barrier, inc=1, device_id={"ep": (ep + k) % n_ep}, device_id_type=MESH)
        return carry

    loads = [
        (xm_hbm, xm), (wo_hbm, wo.at[tp]), (xa_hbm, xa), (wq_hbm, wqkv.at[:, 0:qw]), (wk_hbm, wqkv.at[:, qw:qw + kw]),
        (wv_hbm, wqkv.at[:, qw + kw:qw + 2 * kw]),
        (wg_hbm.at[0], wg), (wu_hbm.at[0], wu), (wd_hbm.at[0], wd),
    ]
    loads = [pltpu.make_async_copy(s, d, load_sem.at[i]) for i, (s, d) in enumerate(loads)]
    loads[0].start()
    lax.fori_loop(1, n_ep, greet, 0)
    for side in (left, right, opp):
        pl.semaphore_signal(barrier, inc=1, device_id={"tp": side}, device_id_type=MESH)
    for copy in loads[1:]:
        copy.start()

    ids = [routes_ref[k:k + 1, :] for k in range(2)]
    experts = iota((n_ep, tok_m), 0)
    tri = jnp.where(iota((tok_m, tok_m), 0) < iota((tok_m, tok_m), 1), 1.0, 0.0).astype(BF)
    slot_row = []
    base = None
    for r in ids:
        hot = experts == r
        hot_b = jnp.where(hot, 1.0, 0.0).astype(BF)
        ranks = dot(hot_b, tri)
        if base is None:
            base = jnp.sum(hot_b.astype(F32), axis=1, keepdims=True)
        else:
            ranks = ranks + base
        rank = jnp.sum(jnp.where(hot, ranks, 0.0), axis=0, keepdims=True).astype(jnp.int32)
        dz = lax.rem((r // npl) - z + nz, nz)
        index = jnp.zeros_like(r)
        for i, d in enumerate(order):
            index = jnp.where(dz == d, i, index)
        place = lax.rem(r, npl)
        inside = jnp.where(rank < MAIN, place * MAIN + rank, main_rows + place * EXTRA + rank - MAIN)
        slot_row.append(index * chunk + inside)

    loads[0].wait()
    col0 = pl.multiple_of(tp * qd, 128)

    def norm_m(b, carry):
        rows = pl.ds(pl.multiple_of(b * 32, 32), 32)
        v = xm[rows, :].astype(F32)
        scale = lax.rsqrt(jnp.mean(v * v, axis=-1, keepdims=True) + epsilon)
        own[rows, :] = (v * scale * egain_ref[...]).astype(BF)
        return carry

    lax.fori_loop(0, tok_m // 32, norm_m, 0)
    loads[1].wait()
    pl.semaphore_wait(barrier, n_ep - 1 + 3)

    def delta(i):
        code = sum(d << (3 * k) for k, d in enumerate(order))
        return lax.rem(lax.shift_right_logical(jnp.int32(code), 3 * i), 8)

    def fold_ext(e, blocks):
        n = npl * EXTRA * blocks
        total = jnp.zeros((n, 128), F32)
        r = iota((n, ext_rows), 0)
        c = iota((n, ext_rows), 1)
        for j in range(blocks):
            pick = jnp.where((r // blocks == c) & (lax.rem(r, blocks) == j), 1.0, 0.0).astype(BF)
            total = total + dot(pick, e[:, j * 128:(j + 1) * 128])
        return total.reshape(npl, EXTRA * blocks, 128).astype(BF)

    def unfold_ext(x, blocks):
        n = npl * EXTRA * blocks
        flat = x.astype(F32).reshape(n, 128).astype(BF)
        r = iota((ext_rows, n), 0)
        c = iota((ext_rows, n), 1)
        out = []
        for j in range(blocks):
            pick = jnp.where(r * blocks + j == c, 1.0, 0.0).astype(BF)
            out.append(dot(pick, flat).astype(BF))
        return out

    def exchange(i, m, main, ext, land_main, land_ext, sems, recv, dest_z):
        def body(k, carry):
            q = lax.rem(p + k, npl)
            dev = {"ep": dest_z * npl + q}
            pltpu.make_async_remote_copy(
                src_ref=main.at[m, pl.ds(pl.multiple_of(q * MAIN, MAIN), MAIN), :],
                dst_ref=land_main, send_sem=sems.at[i, 0], recv_sem=recv.at[i, 0],
                device_id=dev, device_id_type=MESH,
            ).start()
            pltpu.make_async_remote_copy(
                src_ref=ext.at[m, q], dst_ref=land_ext, send_sem=sems.at[i, 1],
                recv_sem=recv.at[i, 1], device_id=dev, device_id_type=MESH,
            ).start()
            return carry

        lax.fori_loop(1 - jnp.minimum(i, 1), npl, body, 0)

    def settle(i, m, main, ext, sems):
        for j, ref in ((0, main), (1, ext)):
            full = ref.at[m]
            few = ref.at[m, 0:(npl - 1) * MAIN, :] if j == 0 else ref.at[m, 0:npl - 1]

            @pl.when(i > 0)
            def _():
                pltpu.make_async_copy(full, full, sems.at[i, j]).wait()

            @pl.when(i == 0)
            def _():
                pltpu.make_async_copy(few, few, sems.at[i, j]).wait()

    my_main = pl.ds(pl.multiple_of(p * MAIN, MAIN), MAIN)
    my_cols = pl.ds(col0, qd)
    lanes_q, lanes_f = qd // 128, width // 128

    def hot_rows(i):
        slot = iota((chunk, tok_m), 0) + i * chunk
        return jnp.where((slot == slot_row[0]) | (slot == slot_row[1]), 1.0, 0.0).astype(BF)

    def full_of(i):
        return jnp.maximum(i - n_ag, 0)

    def dispatch(i, carry):
        rows = dot(hot_rows(i), own[:, my_cols]).astype(BF)
        out_main[i] = rows[0:main_rows]
        out_ext[i] = fold_ext(rows[main_rows:], lanes_q)
        exchange(
            i, i, out_main, out_ext, grid_in.at[i, my_main, my_cols], ext_in.at[i, p],
            disp_s, disp_r, lax.rem(z + delta(i), nz),
        )
        return carry

    def dispatch_full(i, carry):
        d = full_of(i)
        rows = dot(hot_rows(i), own[...]).astype(BF)
        full_main[d] = rows[0:main_rows]
        full_ext[d] = fold_ext(rows[main_rows:], lanes_f)
        exchange(
            i, d, full_main, full_ext, grid_in.at[i, my_main, :], fext_in.at[d, p],
            disp_s, disp_r, lax.rem(z + delta(i), nz),
        )
        return carry

    def start(copies):
        for c in copies:
            c.start()

    def arrived(copies):
        for c in copies:
            c.wait_recv()

    def sent(copies):
        for c in copies:
            c.wait_send()

    def remote(src, dst, sems, recv, dev):
        return pltpu.make_async_remote_copy(
            src_ref=src, dst_ref=dst, send_sem=sems, recv_sem=recv, device_id=dev,
            device_id_type=MESH,
        )

    hw = width // 2
    hrows = qw // 2
    srows = hrows // nx
    my_slice = pl.ds(pl.multiple_of(core * hrows + xc * srows, 16), srows)
    my_half = pl.ds(pl.multiple_of(core * hrows, 16), hrows)

    def wo_own():
        ref = wo.at[tp, my_slice, :]
        return [remote(ref, ref, wo_s.at[k], wo_r.at[k], {"tp": d}) for k, d in ((0, right), (1, left))]

    def wo_fwd():
        a = wo.at[left, my_slice, 0:hw]
        b = wo.at[right, my_slice, hw:width]
        return [
            remote(a, a, wo_s.at[2], wo_r.at[2], {"tp": right}),
            remote(b, b, wo_s.at[3], wo_r.at[3], {"tp": left}),
        ]

    def wo_along():
        out = []
        for k in range(1, nx):
            dev = {"ep": z * npl + lax.rem(xc + k, nx) * 2 + core}
            for shard in (right, left, opp):
                ref = wo.at[shard, my_slice, :]
                out.append(remote(ref, ref, wo_s.at[4], wo_r.at[4], dev))
        return out

    def wo_along_done(sems):
        if nx > 1:
            ref = wo.at[0:3, 0:(nx - 1) * srows, :]
            pltpu.make_async_copy(ref, ref, sems.at[4]).wait()

    def wo_core():
        out = []
        for shard in (right, left, opp):
            ref = wo.at[shard, my_half, :]
            out.append(remote(ref, ref, wo_s.at[5], wo_r.at[5], {"ep": z * npl + xc * 2 + 1 - core}))
        return out

    def wo_core_done(sems):
        ref = wo.at[0:3, 0:hrows, :]
        pltpu.make_async_copy(ref, ref, sems.at[5]).wait()

    start(wo_own())
    lax.fori_loop(1, min(3, n_ag + 1), dispatch, 0)
    dispatch_full(0, 0)
    lax.fori_loop(min(3, n_ag + 1), n_ag + 1, dispatch, 0)
    lax.fori_loop(n_ag + 1, nz, dispatch_full, 0)
    grid_in[0, my_main, :] = full_main[0, my_main, :]
    fext_in[0, p] = full_ext[0, p]
    acc[...] = jnp.zeros_like(acc)

    eye = iota((tok_m, tok_m), 0) == iota((tok_m, tok_m), 1)

    def column(row):
        return jnp.sum(jnp.where(eye, row, 0.0), axis=1, keepdims=True)

    slot_col = [column(r.astype(F32)).astype(jnp.int32) for r in slot_row]
    probs = [prob_ref[k:k + 1, :] for k in range(2)]
    weight_col = [column(gprob_ref[...] * q / (probs[0] + probs[1])) for q in probs]

    def cols(quarter, off, size):
        return pl.ds(pl.multiple_of(quarter * qd + off, 128), size)

    def ag_own(i):
        block = grid_in.at[i, :, my_cols]
        return [
            remote(block, block, ag_s.at[i, s], ag_r.at[i, s], {"tp": d}) for s, d in ((0, right), (1, left))
        ]

    def ag_fwd(i):
        a = grid_in.at[i, :, cols(left, 0, half)]
        b = grid_in.at[i, :, cols(right, half, half)]
        return [
            remote(a, a, ag_s.at[i, 2], ag_r.at[i, 2], {"tp": right}),
            remote(b, b, ag_s.at[i, 3], ag_r.at[i, 3], {"tp": left}),
        ]

    def rs_one(i):
        a = part.at[i, :, cols(opp, 0, half)]
        b = part.at[i, :, cols(opp, half, half)]
        return [
            remote(a, rb1.at[i, 0], rs_s.at[i, 0], rs_r.at[i, 0], {"tp": right}),
            remote(b, rb1.at[i, 1], rs_s.at[i, 1], rs_r.at[i, 1], {"tp": left}),
        ]

    def rs_side(i):
        a = part.at[i, :, cols(right, half, half)]
        b = part.at[i, :, cols(left, 0, half)]
        return [
            remote(a, rb2.at[i, 0, :, half:qd], rs_s.at[i, 2], rs_r.at[i, 2], {"tp": right}),
            remote(b, rb2.at[i, 1, :, 0:half], rs_s.at[i, 3], rs_r.at[i, 3], {"tp": left}),
        ]

    def rs_two(i):
        return [
            remote(sb.at[i, 0], rb2.at[i, 0, :, 0:half], rs_s.at[i, 4], rs_r.at[i, 4], {"tp": right}),
            remote(sb.at[i, 1], rb2.at[i, 1, :, half:qd], rs_s.at[i, 5], rs_r.at[i, 5], {"tp": left}),
        ]

    quarter_rows = tok_a // n_tp

    def rows_of(t):
        return pl.ds(pl.multiple_of(t * quarter_rows, quarter_rows), quarter_rows)

    my_heads = pl.ds(pl.multiple_of(tp * qw, 128), qw)

    def att_send():
        return [
            remote(att.at[rows_of(d), :], att_all.at[:, my_heads], at_s.at[k], at_r.at[k], {"tp": d})
            for k, d in enumerate((right, left, opp))
        ]

    def halo():
        low, high = kv.at[0:WINDOW, :], kv.at[tok_a + WINDOW:tok_a + 2 * WINDOW, :]
        return [
            remote(kv.at[tok_a:tok_a + WINDOW, :], low, halo_s.at[0], halo_r.at[0], {"ep": after}),
            remote(kv.at[WINDOW:2 * WINDOW, :], high, halo_s.at[1], halo_r.at[1], {"ep": before}),
        ]

    half_dim = HEAD_DIM // 2

    def qkv_all():
        for copy in loads[2:6]:
            copy.wait()
        inv = inv_ref[...]
        q_gain = jnp.concatenate([qgain_ref[...]] * 2, axis=1)
        k_gain = jnp.concatenate([kgain_ref[...]] * 2, axis=1)
        lane = lax.rem(iota((GRID_W, 128), 1), half_dim)
        is_row = lane < half_dim // 2
        col_ang = iota((GRID_W, 128), 0).astype(F32) * inv
        groups = tok_a // GRID_W
        row_ang = (iota((groups, 128), 0) + ep * groups).astype(F32) * inv
        col_cos, col_sin = jnp.cos(col_ang), jnp.sin(col_ang)
        row_cos, row_sin = jnp.cos(row_ang), jnp.sin(row_ang)
        first = lax.rem(iota((1, 128), 1), HEAD_DIM) < half_dim
        sign = jnp.where(first, -1.0, 1.0)
        tables = []
        for g in range(groups):
            c = jnp.where(is_row, row_cos[g:g + 1, :], col_cos)
            s = jnp.where(is_row, row_sin[g:g + 1, :], col_sin) * sign
            tables.append((c, s))
        ones = jnp.where(iota((128, 128), 0) // HEAD_DIM == iota((128, 128), 1) // HEAD_DIM, 1.0, 0.0).astype(BF)

        def rotated(v, gain, c, s):
            sq = v * v
            hi = sq.astype(BF)
            lo = (sq - hi.astype(F32)).astype(BF)
            mean = (dot(hi, ones) + dot(lo, ones)) * (1.0 / HEAD_DIM)
            scaled = v * lax.rsqrt(mean + epsilon) * gain
            other = jnp.where(first, pltpu.roll(scaled, 128 - half_dim, 1), pltpu.roll(scaled, half_dim, 1))
            return (scaled * c + other * s).astype(BF)

        blk = 128
        for b in range(tok_a // blk):
            def norm_a(j, carry):
                rows = pl.ds(pl.multiple_of(b * blk + j * 32, 32), 32)
                v = xa[rows, :].astype(F32)
                scale = lax.rsqrt(jnp.mean(v * v, axis=-1, keepdims=True) + epsilon)
                normed[rows, :] = (v * scale * again_ref[...]).astype(BF)
                return carry

            lax.fori_loop(0, blk // 32, norm_a, 0)
            rows = slice(b * blk, (b + 1) * blk)
            proj = dot(normed[rows, :], wqkv[...])
            per = blk // GRID_W
            c = jnp.concatenate([tables[b * per + j][0] for j in range(per)], axis=0)
            s = jnp.concatenate([tables[b * per + j][1] for j in range(per)], axis=0)
            for j in range(qw // 128):
                sl = slice(j * 128, (j + 1) * 128)
                qs[rows, sl] = rotated(proj[:, sl], q_gain, c, s)
            dst = slice(WINDOW + b * blk, WINDOW + (b + 1) * blk)
            kv[dst, 0:kw] = rotated(proj[:, qw:qw + kw], k_gain, c, s)
            kv[dst, kw:2 * kw] = proj[:, qw + kw:qw + 2 * kw].astype(BF)

    kv_local = kw // HEAD_DIM
    group = qw // kw
    total_len = tok_a * n_ep
    span = 3 * WINDOW

    def attend(b):
        row0 = pl.multiple_of(b * WINDOW, WINDOW)
        q_rows = pl.ds(row0, WINDOW)
        k_rows = pl.ds(row0, span)
        gap = iota((WINDOW, span), 1) - iota((WINDOW, span), 0)
        pos = ep * tok_a - WINDOW + row0 + iota((WINDOW, span), 1)
        valid = (gap >= 0) & (gap <= 2 * WINDOW) & (pos >= 0) & (pos < total_len)
        for h in range(kv_local):
            keys = kv[k_rows, h * HEAD_DIM:(h + 1) * HEAD_DIM]
            vals = kv[k_rows, kw + h * HEAD_DIM:kw + (h + 1) * HEAD_DIM]
            for g in range(group):
                head = h * group + g
                lanes = slice(head * HEAD_DIM, (head + 1) * HEAD_DIM)
                q = qs[q_rows, lanes]
                s = lax.dot_general(q, keys, (((1,), (1,)), ((), ())), preferred_element_type=F32)
                s = jnp.where(valid, s * HEAD_DIM ** (-0.5), -1e30)
                sink = sink_ref[head]
                peak = jnp.maximum(jnp.max(s, axis=-1, keepdims=True), sink)
                w = jnp.exp(s - peak)
                denom = jnp.sum(w, axis=-1, keepdims=True) + jnp.exp(sink - peak)
                weights = (w * (1.0 / denom)).astype(BF)
                att[q_rows, lanes] = dot(weights, vals).astype(BF)

    n_blocks = tok_a // WINDOW

    qkv_all()
    start(halo())

    def tick(i, carry):
        @pl.when(i < n_ag)
        def _():
            c = i + 1
            settle(c, c, out_main, ext_in, disp_r)
            for j, piece in enumerate(unfold_ext(ext_in[c], lanes_q)):
                grid_in[c, main_rows:chunk, cols(tp, j * 128, 128)] = piece
            start(ag_own(c))

        @pl.when(i == 0)
        def _():
            arrived(wo_own())
            start(wo_fwd())

        @pl.when((i >= 1) & (i < n_ag + 1))
        def _():
            arrived(ag_own(i))
            start(ag_fwd(i))

        @pl.when(i == 1)
        def _():
            arrived(wo_fwd())
            start(wo_along())

        @pl.when((i >= 1) & (i < nz + 1))
        def _():
            c = i - 1

            @pl.when(c == 0)
            def _():
                for copy in loads[6:9]:
                    copy.wait()

            direct = (c == 0) | (c > n_ag)

            @pl.when(direct)
            def _():
                d = full_of(c)
                settle(c, d, full_main, fext_in, disp_r)
                for j, piece in enumerate(unfold_ext(fext_in[d], lanes_f)):
                    grid_in[c, main_rows:chunk, j * 128:(j + 1) * 128] = piece

            @pl.when(jnp.logical_not(direct))
            def _():
                arrived(ag_fwd(c))

            x = grid_in[c]
            g = dot(x, wg[...])
            u = dot(x, wu[...])
            hidden = (g / (1.0 + jnp.exp(-g)) * u).astype(BF)
            part[c] = dot(hidden, wd[...]).astype(BF)
            start(rs_one(c))
            start(rs_side(c))

        @pl.when((i >= 2) & (i < nz + 2))
        def _():
            c = i - 2
            arrived(rs_one(c))
            for s, (quarter, off) in enumerate(((right, 0), (left, half))):
                mine = part[c, :, cols(quarter, off, half)].astype(F32)
                sb[c, s] = (mine + rb1[c, s].astype(F32)).astype(BF)
            start(rs_two(c))

        @pl.when((i >= 3) & (i < nz + 3))
        def _():
            c = i - 3
            arrived(rs_side(c))
            arrived(rs_two(c))
            total = part[c, :, my_cols].astype(F32) + rb2[c, 0].astype(F32) + rb2[c, 1].astype(F32)
            total = total.astype(BF)
            res_main[c] = total[0:main_rows]
            res_ext[c] = fold_ext(total[main_rows:], lanes_q)
            exchange(
                c, c, res_main, res_ext, back_main.at[c, my_main, :], back_ext.at[c, p],
                ret_s, ret_r, lax.rem(z - delta(c) + nz, nz),
            )

            @pl.when(c == 0)
            def _():
                back_main[0, my_main, :] = res_main[0, my_main, :]
                back_ext[0, p] = res_ext[0, p]

        @pl.when(i == FIRST_ATT)
        def _():
            arrived(halo())

        @pl.when((i >= FIRST_ATT) & (i < FIRST_ATT + n_blocks))
        def _():
            attend(i - FIRST_ATT)

        last_att = FIRST_ATT + n_blocks - 1

        @pl.when(i == last_att)
        def _():
            start(att_send())
            wo_along_done(wo_r)
            start(wo_core())
            att_all[:, my_heads] = att[rows_of(tp), :]

        @pl.when(i == last_att + 2)
        def _():
            arrived(att_send())
            wo_core_done(wo_r)
            total = dot(att_all[:, 0:qw], wo[0])
            for t in range(1, n_tp):
                total = total + dot(att_all[:, t * qw:(t + 1) * qw], wo[t])
            attend_ref[...] = total.astype(BF)

        @pl.when(i >= LAG)
        def _():
            c = i - LAG
            settle(c, c, back_main, back_ext, ret_r)
            e = unfold_ext(back_ext[c], lanes_q)
            slot = iota((tok_m, chunk), 1) + c * chunk
            for k in range(2):
                hot = jnp.where(slot == slot_col[k], 1.0, 0.0).astype(BF)
                acc[k] += dot(hot[:, 0:main_rows], back_main[c])
                for j, piece in enumerate(e):
                    sl = slice(j * 128, (j + 1) * 128)
                    acc[k, :, sl] += dot(hot[:, main_rows:], piece)

        return carry

    lax.fori_loop(0, max(nz + LAG, FIRST_ATT + n_blocks + 2), tick, 0)
    expert_ref[...] = (acc[0] * weight_col[0] + acc[1] * weight_col[1]).astype(BF)

    def drain(i, carry):
        settle(i, i, res_main, res_ext, ret_s)
        for stage in (rs_one, rs_side, rs_two):
            sent(stage(i))
        return carry

    def drain_ag(i, carry):
        settle(i, i, out_main, out_ext, disp_s)
        for stage in (ag_own, ag_fwd):
            sent(stage(i))
        return carry

    def drain_full(i, carry):
        settle(i, full_of(i), full_main, full_ext, disp_s)
        return carry

    lax.fori_loop(0, nz, drain, 0)
    lax.fori_loop(1, n_ag + 1, drain_ag, 0)
    drain_full(0, 0)
    lax.fori_loop(n_ag + 1, nz, drain_full, 0)
    for stage in (halo, wo_own, wo_fwd, att_send):
        sent(stage())
    wo_along_done(wo_s)
    wo_core_done(wo_s)


def fused(dims, *args):
    nz, npl, n_tp, tok_m, tok_a, width, ff, qw, kw = dims
    n_full = nz - ORDERS[nz][1]
    qd = width // n_tp
    half = qd // 2
    chunk = npl * (MAIN + EXTRA)
    eb = EXTRA * qd // 128
    qr = tok_a // n_tp
    vm = pltpu.VMEM
    dma = pltpu.SemaphoreType.DMA
    any_spec = pl.BlockSpec(memory_space=pl.ANY)
    vmem_spec = pl.BlockSpec(memory_space=pltpu.VMEM)
    smem_spec = pl.BlockSpec(memory_space=pltpu.SMEM)
    return pl.pallas_call(
        functools.partial(kernel, dims),
        out_shape=(
            jax.ShapeDtypeStruct((qr, width), BF),
            jax.ShapeDtypeStruct((tok_m, qd), BF),
        ),
        in_specs=[vmem_spec] * 8 + [smem_spec] + [any_spec] * 9,
        out_specs=(vmem_spec, vmem_spec),
        scratch_shapes=[
            vm((tok_m, width), BF), vm((width, ff), BF), vm((width, ff), BF), vm((ff, width), BF),
            vm((tok_a, width), BF), vm((width, qw + 2 * kw), BF), vm((n_tp, qw, width), BF),
            vm((tok_m, width), BF),
            vm((nz, npl * MAIN, qd), BF), vm((nz, npl, eb, 128), BF),
            vm((n_full, npl * MAIN, width), BF), vm((n_full, npl, eb * n_tp, 128), BF),
            vm((nz, chunk, width), BF), vm((nz, npl, eb, 128), BF), vm((n_full, npl, eb * n_tp, 128), BF),
            vm((nz, chunk, width), BF),
            vm((nz, 2, chunk, half), BF), vm((nz, 2, chunk, half), BF), vm((nz, 2, chunk, qd), BF),
            vm((nz, npl * MAIN, qd), BF), vm((nz, npl, eb, 128), BF),
            vm((nz, npl * MAIN, qd), BF), vm((nz, npl, eb, 128), BF),
            vm((2, tok_m, qd), F32),
            vm((tok_a, width), BF), vm((tok_a, qw), BF), vm((tok_a + 2 * WINDOW, 2 * kw), BF),
            vm((tok_a, qw), BF), vm((qr, qw * n_tp), BF),
            dma((9,)), dma((nz, 2)), dma((nz, 2)), dma((nz, 2)), dma((nz, 2)),
            dma((nz, 4)), dma((nz, 4)), dma((nz, 6)), dma((nz, 6)),
            dma((2,)), dma((2,)), dma((6,)), dma((6,)), dma((3,)), dma((3,)),
        ],
        compiler_params=pltpu.CompilerParams(
            collective_id=0, has_side_effects=True, vmem_limit_bytes=60 * 1024 * 1024
        ),
        name="fused_layer",
    )(*args)


def per_device(
    planes,
    x_attend, attend_gain, w_query, w_key, w_value, query_gain, key_gain, sink_logit, w_output,
    x_experts, expert_gain, routes, group_prob, expert_prob, w_gate, w_up, w_down,
):
    n_ep, n_tp = lax.axis_size("ep"), lax.axis_size("tp")
    tok_a, width = x_attend.shape
    dims = (
        planes, n_ep // planes, n_tp, x_experts.shape[0], tok_a, width, w_gate.shape[2],
        w_query.shape[1], w_key.shape[1],
    )
    half_dim = HEAD_DIM // 2
    inverse = np.float32(rope_base) ** (-np.arange(0, half_dim, 2, dtype=np.float32) / np.float32(half_dim))
    inverse = np.tile(inverse.astype(np.float32), 256 // half_dim)[None, :]
    return fused(
        dims, routes.T, expert_prob.T, group_prob[None, :], expert_gain[None, :], attend_gain[None, :],
        query_gain[None, :], key_gain[None, :], inverse,
        sink_logit, x_experts, w_gate, w_up, w_down, x_attend, w_query, w_key, w_value, w_output,
    )


def solution(mesh, planes=8):
    placed = (
        P("ep", None), P(), P(None, "tp"), P(None, "tp"), P(None, "tp"), P(), P(), P("tp"),
        P("tp", None), P("ep", None), P(), P("ep", None), P("ep"), P("ep", None),
        P("ep", None, "tp"), P("ep", None, "tp"), P("ep", "tp", None),
    )
    return jax.shard_map(
        functools.partial(per_device, planes),
        mesh=mesh,
        in_specs=placed,
        out_specs=(P(("ep", "tp"), None), P("ep", "tp")),
        check_vma=False,
    )
```

time: 158 us -> 125 us (0.79)
  Pallas kernels: 149 us -> 120 us
  other arithmetic: 2.14 us -> 0 us
  local copies, waits for them, and re-layouts: 6.85 us -> 4.89 us
    pallas_call x1, Pallas kernels: 149 us -> 120 us  [fused(): pl.pallas_call(functools.partial(kernel, dims), out_shape=(jax.ShapeDtype...]
    unnamed x3 -> x2, local copies, waits for them, and re-layouts: 5.15 us -> 3.65 us
where the time goes in v2:
time: 125 us
  Pallas kernels  120 us (96%)
  local copies, waits for them, and re-layouts  4.89 us (4%)
    pallas_call x1, Pallas kernels, fused(): pl.pallas_call(functools.partial(kernel, dims), out_shape=(jax.ShapeDtype...  120 us
    unnamed x2, local copies, waits for them, and re-layouts  3.65 us

profile of v2, /device:TPU:1, one launch (start us, length us, event | category | flops | bytes accessed | tf_op | source)
XLA Modules:
  0.0 125.2 jit_solution(12349018398399090157)
XLA Ops:
  0.6 1.2 broadcast_in_dim.15.refs_2_
  1.9 119.7 %fused_layer.1 = (bf16[128,2048]{1,0:T(8,128)(2,1)}, bf16[384,512]{1,0:T(8,128)(2,1)}) custom-call(s32[2,384]{1,0:T(2,128)} %bitcast.8, f32[2,384]{1,0:T(2,128)} %bitcast.9, f32[1,384]{1,0:T(1,128)} %broadcast_in_dim.15.refs_2_, f32[1,2048]{1,0:T(1,128)} %bitcast.6, f32[1,2048]{1,0:T(1,128)} %bitcast.7, f32[1,64]{1,0:T(1,128)} %bitcast.10, ...), custom_call_target="tpu_custom_call" | custom-call | tf_op jit(solution)/shard_map/fused_layer/pallas_call | solution.py:598
  121.6 1.9 %copy.22 = bf16[128,2048]{1,0:T(8,128)(2,1)} copy(bf16[128,2048]{1,0:T(8,128)(2,1)} %get-tuple-element.4) | data formatting | bytes 1048576
  123.5 1.8 %copy.23 = bf16[384,512]{1,0:T(8,128)(2,1)} copy(bf16[384,512]{1,0:T(8,128)(2,1)} %get-tuple-element.5) | data formatting | bytes 786432

commit v3 on v2

--- a/solution.py
+++ b/solution.py
@@ -14,7 +14,7 @@
 MAIN = 16
 EXTRA = 2
 FIRST_ATT = 3
-LAG = 4
+LAG = 7
 
 epsilon = 1e-06
 rope_base = 10000.0
@@ -32,7 +32,7 @@
     return lax.broadcasted_iota(jnp.int32, shape, dim)
 
 
-ORDERS = {8: ((0, 2, 6, 5, 4, 3, 7, 1), 5), 4: ((0, 2, 3, 1), 1), 2: ((0, 1), 1)}
+ORDERS = {8: ((0, 3, 5, 4, 6, 2, 1, 7), 5), 4: ((0, 2, 1, 3), 2), 2: ((0, 1), 1)}
 
 
 def kernel(dims, *refs):
@@ -42,9 +42,9 @@
         xm_hbm, wg_hbm, wu_hbm, wd_hbm, xa_hbm, wq_hbm, wk_hbm, wv_hbm, wo_hbm,
         attend_ref, expert_ref,
         xm, wg, wu, wd, xa, wqkv, wo,
-        own, out_main, out_ext, full_main, full_ext, grid_in, ext_in, fext_in, part, rb1, sb, rb2,
+        own, out_main, out_ext, full_main, full_ext, grid_in, ext_in, fext_in, hid, wdq, relay,
         res_main, res_ext, back_main, back_ext, acc, normed, qs, kv, att, att_all,
-        load_sem, disp_s, disp_r, ret_s, ret_r, ag_s, ag_r, rs_s, rs_r, halo_s, halo_r, wo_s, wo_r, at_s, at_r,
+        load_sem, disp_s, disp_r, ret_s, ret_r, ag_s, ag_r, hg_s, hg_r, halo_s, halo_r, wo_s, wo_r, at_s, at_r, wd_s, wd_r,
     ) = refs
     order, n_ag = ORDERS[nz]
     qd = width // n_tp
@@ -69,9 +69,9 @@
         return carry
 
     loads = [
-        (xm_hbm, xm), (wo_hbm, wo.at[tp]), (xa_hbm, xa), (wq_hbm, wqkv.at[:, 0:qw]), (wk_hbm, wqkv.at[:, qw:qw + kw]),
+        (xm_hbm, xm), (wd_hbm.at[0], wd), (wo_hbm, wo.at[tp]), (xa_hbm, xa), (wq_hbm, wqkv.at[:, 0:qw]), (wk_hbm, wqkv.at[:, qw:qw + kw]),
         (wv_hbm, wqkv.at[:, qw + kw:qw + 2 * kw]),
-        (wg_hbm.at[0], wg), (wu_hbm.at[0], wu), (wd_hbm.at[0], wd),
+        (wg_hbm.at[0], wg), (wu_hbm.at[0], wu),
     ]
     loads = [pltpu.make_async_copy(s, d, load_sem.at[i]) for i, (s, d) in enumerate(loads)]
     loads[0].start()
@@ -115,6 +115,7 @@
 
     lax.fori_loop(0, tok_m // 32, norm_m, 0)
     loads[1].wait()
+    loads[2].wait()
     pl.semaphore_wait(barrier, n_ep - 1 + 3)
 
     def delta(i):
@@ -265,6 +266,28 @@
         ref = wo.at[0:3, 0:hrows, :]
         pltpu.make_async_copy(ref, ref, sems.at[5]).wait()
 
+    def cols(quarter, off, size):
+        return pl.ds(pl.multiple_of(quarter * qd + off, 128), size)
+
+    def wd_rows(t):
+        return pl.ds(pl.multiple_of(t * ff, 128), ff)
+
+    def wd_own():
+        mine = wd_rows(tp)
+        return [
+            remote(wd.at[:, cols(right, 0, qd)], wdq.at[mine, :], wd_s.at[0], wd_r.at[0], {"tp": right}),
+            remote(wd.at[:, cols(left, 0, qd)], wdq.at[mine, :], wd_s.at[1], wd_r.at[1], {"tp": left}),
+            remote(wd.at[:, cols(opp, 0, half)], relay.at[0], wd_s.at[2], wd_r.at[2], {"tp": right}),
+            remote(wd.at[:, cols(opp, half, half)], relay.at[1], wd_s.at[3], wd_r.at[3], {"tp": left}),
+        ]
+
+    def wd_fwd():
+        return [
+            remote(relay.at[0], wdq.at[wd_rows(left), 0:half], wd_s.at[4], wd_r.at[4], {"tp": right}),
+            remote(relay.at[1], wdq.at[wd_rows(right), half:qd], wd_s.at[5], wd_r.at[5], {"tp": left}),
+        ]
+
+    start(wd_own())
     start(wo_own())
     lax.fori_loop(1, min(3, n_ag + 1), dispatch, 0)
     dispatch_full(0, 0)
@@ -281,10 +304,7 @@
 
     slot_col = [column(r.astype(F32)).astype(jnp.int32) for r in slot_row]
     probs = [prob_ref[k:k + 1, :] for k in range(2)]
-    weight_col = [column(gprob_ref[...] * q / (probs[0] + probs[1])) for q in probs]
-
-    def cols(quarter, off, size):
-        return pl.ds(pl.multiple_of(quarter * qd + off, 128), size)
+    weight_col = [column(gprob_ref[...][None, :] * q / (probs[0] + probs[1])) for q in probs]
 
     def ag_own(i):
         block = grid_in.at[i, :, my_cols]
@@ -300,26 +320,23 @@
             remote(b, b, ag_s.at[i, 3], ag_r.at[i, 3], {"tp": left}),
         ]
 
-    def rs_one(i):
-        a = part.at[i, :, cols(opp, 0, half)]
-        b = part.at[i, :, cols(opp, half, half)]
-        return [
-            remote(a, rb1.at[i, 0], rs_s.at[i, 0], rs_r.at[i, 0], {"tp": right}),
-            remote(b, rb1.at[i, 1], rs_s.at[i, 1], rs_r.at[i, 1], {"tp": left}),
-        ]
-
-    def rs_side(i):
-        a = part.at[i, :, cols(right, half, half)]
-        b = part.at[i, :, cols(left, 0, half)]
-        return [
-            remote(a, rb2.at[i, 0, :, half:qd], rs_s.at[i, 2], rs_r.at[i, 2], {"tp": right}),
-            remote(b, rb2.at[i, 1, :, 0:half], rs_s.at[i, 3], rs_r.at[i, 3], {"tp": left}),
-        ]
-
-    def rs_two(i):
-        return [
-            remote(sb.at[i, 0], rb2.at[i, 0, :, 0:half], rs_s.at[i, 4], rs_r.at[i, 4], {"tp": right}),
-            remote(sb.at[i, 1], rb2.at[i, 1, :, half:qd], rs_s.at[i, 5], rs_r.at[i, 5], {"tp": left}),
+    hf = ff // 2
+
+    def units(t, off, size):
+        return pl.ds(pl.multiple_of(t * ff + off, 128), size)
+
+    def hg_own(i):
+        block = hid.at[i, :, units(tp, 0, ff)]
+        return [
+            remote(block, block, hg_s.at[i, s], hg_r.at[i, s], {"tp": d}) for s, d in ((0, right), (1, left))
+        ]
+
+    def hg_fwd(i):
+        a = hid.at[i, :, units(left, 0, hf)]
+        b = hid.at[i, :, units(right, hf, hf)]
+        return [
+            remote(a, a, hg_s.at[i, 2], hg_r.at[i, 2], {"tp": right}),
+            remote(b, b, hg_s.at[i, 3], hg_r.at[i, 3], {"tp": left}),
         ]
 
     quarter_rows = tok_a // n_tp
@@ -345,7 +362,7 @@
     half_dim = HEAD_DIM // 2
 
     def qkv_all():
-        for copy in loads[2:6]:
+        for copy in loads[3:7]:
             copy.wait()
         inv = inv_ref[...]
         q_gain = jnp.concatenate([qgain_ref[...]] * 2, axis=1)
@@ -430,6 +447,9 @@
     qkv_all()
     start(halo())
 
+    def staged(i, lag):
+        return (i == lag - 1) | ((i > lag) & (i < nz + lag)), jnp.maximum(i - lag, 0)
+
     def tick(i, carry):
         @pl.when(i < n_ag)
         def _():
@@ -441,6 +461,9 @@
 
         @pl.when(i == 0)
         def _():
+            arrived(wd_own())
+            start(wd_fwd())
+            wdq[wd_rows(tp), :] = wd[:, my_cols]
             arrived(wo_own())
             start(wo_fwd())
 
@@ -454,13 +477,15 @@
             arrived(wo_fwd())
             start(wo_along())
 
-        @pl.when((i >= 1) & (i < nz + 1))
-        def _():
-            c = i - 1
+        ffn_on, ffn_c = staged(i, 1)
+
+        @pl.when(ffn_on)
+        def _():
+            c = ffn_c
 
             @pl.when(c == 0)
             def _():
-                for copy in loads[6:9]:
+                for copy in loads[7:9]:
                     copy.wait()
 
             direct = (c == 0) | (c > n_ag)
@@ -479,27 +504,28 @@
             x = grid_in[c]
             g = dot(x, wg[...])
             u = dot(x, wu[...])
-            hidden = (g / (1.0 + jnp.exp(-g)) * u).astype(BF)
-            part[c] = dot(hidden, wd[...]).astype(BF)
-            start(rs_one(c))
-            start(rs_side(c))
-
-        @pl.when((i >= 2) & (i < nz + 2))
-        def _():
-            c = i - 2
-            arrived(rs_one(c))
-            for s, (quarter, off) in enumerate(((right, 0), (left, half))):
-                mine = part[c, :, cols(quarter, off, half)].astype(F32)
-                sb[c, s] = (mine + rb1[c, s].astype(F32)).astype(BF)
-            start(rs_two(c))
-
-        @pl.when((i >= 3) & (i < nz + 3))
-        def _():
-            c = i - 3
-            arrived(rs_side(c))
-            arrived(rs_two(c))
-            total = part[c, :, my_cols].astype(F32) + rb2[c, 0].astype(F32) + rb2[c, 1].astype(F32)
-            total = total.astype(BF)
+            hid[c, :, units(tp, 0, ff)] = (g / (1.0 + jnp.exp(-g)) * u).astype(BF)
+            start(hg_own(c))
+
+        mid_on, mid_c = staged(i, 2)
+
+        @pl.when(mid_on)
+        def _():
+            c = mid_c
+            arrived(hg_own(c))
+            start(hg_fwd(c))
+
+        fin_on, fin_c = staged(i, 3)
+
+        @pl.when(fin_on)
+        def _():
+            c = fin_c
+            @pl.when(c == 0)
+            def _():
+                arrived(wd_fwd())
+
+            arrived(hg_fwd(c))
+            total = dot(hid[c], wdq[...]).astype(BF)
             res_main[c] = total[0:main_rows]
             res_ext[c] = fold_ext(total[main_rows:], lanes_q)
             exchange(
@@ -558,7 +584,7 @@
 
     def drain(i, carry):
         settle(i, i, res_main, res_ext, ret_s)
-        for stage in (rs_one, rs_side, rs_two):
+        for stage in (hg_own, hg_fwd):
             sent(stage(i))
         return carry
 
@@ -576,7 +602,7 @@
     lax.fori_loop(1, n_ag + 1, drain_ag, 0)
     drain_full(0, 0)
     lax.fori_loop(n_ag + 1, nz, drain_full, 0)
-    for stage in (halo, wo_own, wo_fwd, att_send):
+    for stage in (halo, wo_own, wo_fwd, wd_own, wd_fwd, att_send):
         sent(stage())
     wo_along_done(wo_s)
     wo_core_done(wo_s)
@@ -597,10 +623,7 @@
     smem_spec = pl.BlockSpec(memory_space=pltpu.SMEM)
     return pl.pallas_call(
         functools.partial(kernel, dims),
-        out_shape=(
-            jax.ShapeDtypeStruct((qr, width), BF),
-            jax.ShapeDtypeStruct((tok_m, qd), BF),
-        ),
+        out_shape=(pltpu.VMEM((qr, width), BF), pltpu.VMEM((tok_m, qd), BF)),
         in_specs=[vmem_spec] * 8 + [smem_spec] + [any_spec] * 9,
         out_specs=(vmem_spec, vmem_spec),
         scratch_shapes=[
@@ -610,16 +633,15 @@
             vm((nz, npl * MAIN, qd), BF), vm((nz, npl, eb, 128), BF),
             vm((n_full, npl * MAIN, width), BF), vm((n_full, npl, eb * n_tp, 128), BF),
             vm((nz, chunk, width), BF), vm((nz, npl, eb, 128), BF), vm((n_full, npl, eb * n_tp, 128), BF),
-            vm((nz, chunk, width), BF),
-            vm((nz, 2, chunk, half), BF), vm((nz, 2, chunk, half), BF), vm((nz, 2, chunk, qd), BF),
+            vm((nz, chunk, ff * n_tp), BF), vm((ff * n_tp, qd), BF), vm((2, ff, half), BF),
             vm((nz, npl * MAIN, qd), BF), vm((nz, npl, eb, 128), BF),
             vm((nz, npl * MAIN, qd), BF), vm((nz, npl, eb, 128), BF),
             vm((2, tok_m, qd), F32),
             vm((tok_a, width), BF), vm((tok_a, qw), BF), vm((tok_a + 2 * WINDOW, 2 * kw), BF),
             vm((tok_a, qw), BF), vm((qr, qw * n_tp), BF),
             dma((9,)), dma((nz, 2)), dma((nz, 2)), dma((nz, 2)), dma((nz, 2)),
-            dma((nz, 4)), dma((nz, 4)), dma((nz, 6)), dma((nz, 6)),
-            dma((2,)), dma((2,)), dma((6,)), dma((6,)), dma((3,)), dma((3,)),
+            dma((nz, 4)), dma((nz, 4)), dma((nz, 4)), dma((nz, 4)),
+            dma((2,)), dma((2,)), dma((6,)), dma((6,)), dma((3,)), dma((3,)), dma((6,)), dma((6,)),
         ],
         compiler_params=pltpu.CompilerParams(
             collective_id=0, has_side_effects=True, vmem_limit_bytes=60 * 1024 * 1024
@@ -643,7 +665,7 @@
     inverse = np.float32(rope_base) ** (-np.arange(0, half_dim, 2, dtype=np.float32) / np.float32(half_dim))
     inverse = np.tile(inverse.astype(np.float32), 256 // half_dim)[None, :]
     return fused(
-        dims, routes.T, expert_prob.T, group_prob[None, :], expert_gain[None, :], attend_gain[None, :],
+        dims, routes.T, expert_prob.T, group_prob, expert_gain[None, :], attend_gain[None, :],
         query_gain[None, :], key_gain[None, :], inverse,
         sink_logit, x_experts, w_gate, w_up, w_down, x_attend, w_query, w_key, w_value, w_output,
     )

time: 125 us -> 97.4 us (0.78)
  Pallas kernels: 120 us -> 95.1 us
  local copies, waits for them, and re-layouts: 4.89 us -> 1.54 us
    pallas_call x1, Pallas kernels: 120 us -> 95.1 us  [fused(): pl.pallas_call(functools.partial(kernel, dims), out_shape=(pltpu.VMEM((qr...]
    unnamed x2, local copies, waits for them, and re-layouts: 3.65 us -> 1.54 us
where the time goes in v3:
time: 97.4 us; the launch traced here: 97.3 us
  Pallas kernels  95.1 us (98%)
  local copies, waits for them, and re-layouts  1.54 us (2%)
    pallas_call x1, Pallas kernels, fused(): pl.pallas_call(functools.partial(kernel, dims), out_shape=(pltpu.VMEM((qr...  95.1 us

profile of v3, /device:TPU:1, one launch (start us, length us, event | category | flops | bytes accessed | tf_op | source)
XLA Modules:
  0.0 97.3 jit_solution(3375131302995620801)
XLA Ops:
  0.6 95.1 %fused_layer.1 = (bf16[128,2048]{1,0:T(8,128)(2,1)S(1)}, bf16[384,512]{1,0:T(8,128)(2,1)S(1)}) custom-call(s32[2,384]{1,0:T(2,128)} %bitcast.8, f32[2,384]{1,0:T(2,128)} %bitcast.9, f32[384]{0:T(512)} %refs_2_.1, f32[1,2048]{1,0:T(1,128)} %bitcast.6, f32[1,2048]{1,0:T(1,128)} %bitcast.7, f32[1,64]{1,0:T(1,128)} %bitcast.10, f32[1,64]{1,0:T(1,128)} %bitcast.11, ...), custom_call_target="tpu_custom_call" | custom-call | tf_op jit(solution)/shard_map/fused_layer/pallas_call | solution.py:624
  95.8 0.8 copy.22
  96.6 0.7 copy.23
